TPU v7x, 128 devices: a whole 4x4x4 slice. The times are simulated.
128 devices in a mesh: sp: 16 (over z, y), dp: 8 (over x, core).
Axes of the slice: x: 4, y: 4, z: 4, core: 2. Of those that a mesh axis runs over, the one named last changes fastest.
Arguments:
- skip_connection_stream: bfloat16 [8, 2048, 2048], P('dp', 'sp'), may hold values from -6 to 6
- emitted_valve_unscaled: bfloat16 [8, 2048, 1024], P('dp', 'sp'), may hold values from -6 to 6
- channel_source_mapped: bfloat16 [8, 2048, 1024], P('dp', 'sp'), may hold values from -6 to 6
- hidden_source_mapped: bfloat16 [8, 2048, 256], P('dp', 'sp'), may hold values from -6 to 6
- probe_mapped_values: bfloat16 [8, 2048, 256], P('dp', 'sp'), may hold values from -6 to 6
- increment_premapped: float32 [8, 2048, 16], P('dp', None, 'sp'), may hold values from -6 to 6
- extra_log_fading: float32 [8, 2048, 16], P('dp', None, 'sp'), may hold values from -2 to 0
- channel_fading_speed: float32 [16], replicated, may hold values from 0 to 1, as said below
- channel_source_kernel: float32 [4, 1024], replicated, may hold values from -3 to 3
- hidden_source_kernel: float32 [4, 256], replicated, may hold values from -3 to 3
- probe_kernel_coefficients: float32 [4, 256], replicated, may hold values from -3 to 3
- cluster_scaling_factor: float32 [1024], replicated, may hold values from 0.1 to 1.9
- emitted_mapping_matrix: bfloat16 [1024, 2048], replicated, may hold values from -0.1875 to 0.1875
- standardize_scaling: float32 [2048], replicated, may hold values from 0.1 to 1.9
- standardize_offset: float32 [2048], replicated, may hold values from -2 to 2
- chosen_specialist_ids: int32 [8, 2048, 2], P('dp', 'sp'), may hold values from 0 to 15, all different within a row; in each aligned block of 128 rows (0 to 127, 128 to 255, ..., all dimensions but the last counted through in order) at most 24 rows name the same one
- specialist_mixing_shares: float32 [8, 2048, 2], P('dp', 'sp'), may hold values from 0.2 to 1
- specialist_gating_matrices: bfloat16 [16, 2048, 5120], P('sp', None, 'dp'), may hold values from -0.125 to 0.125
- raising_matrices: bfloat16 [16, 2048, 5120], P('sp', None, 'dp'), may hold values from -0.125 to 0.125
- lowering_matrices: bfloat16 [16, 5120, 2048], P('sp', 'dp'), may hold values from -0.078125 to 0.078125
Outputs:
- layer_out: bfloat16 [8, 2048, 2048], P('dp', 'sp')
Inputs may be any that keep to these rules, and one draw needn't show every extreme that they name: `chosen_specialist_ids`: each row names two different experts. The rows of one device name no expert more than 24 times, a bound that some block reaches. `channel_fading_speed`: Positive.
All inputs are finite; a program needn't handle non-finite values.
Results may differ from a plain program's by a relative error of at most 0.015.
Values may be sent and summed in bfloat16 or wider, within the bound.
A program may use at most 128 MiB of HBM per device.

v0:
```python
import jax
import jax.numpy as jnp
from jax import lax
from jax.experimental import pallas as pl
from jax.experimental.pallas import tpu as pltpu
from jax.sharding import PartitionSpec as P

HEADS = 16
HEAD_DIM = 64
GROUPS = 4
STATE = 64
KERNEL = 4
BLK = 128


rms_eps = 1e-06
norm_eps = 1e-05


MESH = pl.DeviceIdType.MESH


def expert_kernel(
    rows, gate_w, raise_w, lower_w, out,
    gathered, partial, relayed, summed, gate_v, raise_v, lower_v, hidden,
    weight_sem, weight_send, weight_recv, go_send, go_recv, ring_send, ring_recv,
    sum_send, sum_recv, back_send, back_recv,
):
    sp = lax.axis_index("sp")
    dp = lax.axis_index("dp")
    z, y = lax.div(sp, 4), lax.rem(sp, 4)
    x, core = lax.div(dp, 2), lax.rem(dp, 2)
    right = (sp, lax.rem(x + 1, 4) * 2 + core)
    left = (sp, lax.rem(x + 3, 4) * 2 + core)
    twin = (sp, x * 2 + 1 - core)
    width = rows.shape[2]
    part = gate_w.shape[1]

    def ahead(o):
        return lax.rem(z + lax.div(o, 4), 4) * 4 + lax.rem(y + lax.rem(o, 4), 4)

    def behind(o):
        return lax.rem(z + 4 - lax.div(o, 4), 4) * 4 + lax.rem(y + 4 - lax.rem(o, 4), 4)

    barrier = pltpu.get_barrier_semaphore()

    def greet(o, carry):
        pl.semaphore_signal(barrier, inc=1, device_id=(ahead(o), dp), device_id_type=MESH)
        return carry

    lax.fori_loop(1, 16, greet, 0)
    for friend in (left, right, twin):
        pl.semaphore_signal(barrier, inc=1, device_id=friend, device_id_type=MESH)
    pl.semaphore_wait(barrier, 18)

    def go(o):
        return pltpu.make_async_remote_copy(
            src_ref=rows.at[pl.ds(3 * ahead(o), 3)],
            dst_ref=gathered.at[0, pl.ds(3 * o, 3)],
            send_sem=go_send.at[o],
            recv_sem=go_recv.at[o],
            device_id=(ahead(o), dp),
            device_id_type=MESH,
        )

    own_rows = pltpu.make_async_copy(
        rows.at[pl.ds(3 * sp, 3)], gathered.at[0, pl.ds(0, 3)], go_send.at[0]
    )
    own_rows.start()

    def start_go(o, carry):
        go(o).start()
        return carry

    lax.fori_loop(1, 16, start_go, 0)
    loads, gifts = [], []
    for k, (source, target) in enumerate(
        ((gate_w, gate_v), (raise_w, raise_v), (lower_w, lower_v))
    ):
        if k < 2:
            mine, theirs = target.at[:, pl.ds(0, part)], target.at[:, pl.ds(part, part)]
        else:
            mine, theirs = target.at[pl.ds(0, part)], target.at[pl.ds(part, part)]
        loads.append(pltpu.make_async_copy(source, mine, weight_sem.at[k]))
        gifts.append(
            pltpu.make_async_remote_copy(
                src_ref=source,
                dst_ref=theirs,
                send_sem=weight_send.at[k],
                recv_sem=weight_recv.at[k],
                device_id=twin,
                device_id_type=MESH,
            )
        )
    for copy in loads + gifts:
        copy.start()

    def group(g):
        return pl.ds(12 * g, 12)

    def ring(src_slot, dst_slot, g, target, lane):
        return pltpu.make_async_remote_copy(
            src_ref=gathered.at[src_slot, group(g)],
            dst_ref=gathered.at[dst_slot, group(g)],
            send_sem=ring_send.at[lane, g],
            recv_sem=ring_recv.at[dst_slot - 1, g],
            device_id=target,
            device_id_type=MESH,
        )

    def to_right(g):
        return ring(0, 1, g, right, 0)

    def to_left(g):
        return ring(0, 2, g, left, 1)

    def onward(g):
        return ring(1, 3, g, right, 2) if g < 2 else ring(2, 3, g, left, 2)

    for g in range(4):
        if g == 0:
            own_rows.wait()

        def wait_go(o, carry):
            go(o).wait_recv()
            return carry

        lax.fori_loop(max(4 * g, 1), 4 * g + 4, wait_go, 0)
        to_right(g).start()
        to_left(g).start()

    for copy in loads:
        copy.wait()
    for copy in gifts:
        copy.wait()

    tile = 256

    def unit(slot, half):
        rows_here = gathered.at[slot, pl.ds(24 * half, 24)].reshape(192, width)
        block = rows_here[...]

        def up(k, carry):
            cols = pl.ds(pl.multiple_of(k * tile, tile), tile)
            gate_val = jnp.dot(block, gate_v[:, cols], preferred_element_type=jnp.float32)
            up_val = jnp.dot(block, raise_v[:, cols], preferred_element_type=jnp.float32)
            hidden[:, cols] = (jax.nn.silu(gate_val) * up_val).astype(jnp.bfloat16)
            return carry

        lax.fori_loop(0, 2 * part // tile, up, 0)
        target = partial.at[slot, pl.ds(24 * half, 24)].reshape(192, width)

        def down(k, carry):
            cols = pl.ds(pl.multiple_of(k * tile, tile), tile)
            target[:, cols] = jnp.dot(
                hidden[...], lower_v[:, cols], preferred_element_type=jnp.float32
            ).astype(jnp.bfloat16)
            return carry

        lax.fori_loop(0, width // tile, down, 0)

    def sum_direct(slot, g):
        side = 0 if slot == 2 else 1
        return pltpu.make_async_remote_copy(
            src_ref=partial.at[slot, group(g)],
            dst_ref=summed.at[side, group(g)],
            send_sem=sum_send.at[side, g],
            recv_sem=sum_recv.at[side, g],
            device_id=right if slot == 2 else left,
            device_id_type=MESH,
        )

    def sum_relay(g):
        return pltpu.make_async_remote_copy(
            src_ref=partial.at[3, group(g)],
            dst_ref=relayed.at[group(g)],
            send_sem=sum_send.at[2, g],
            recv_sem=sum_recv.at[2, g],
            device_id=right if g < 2 else left,
            device_id_type=MESH,
        )

    unit(0, 0)
    to_right(0).wait_recv()
    onward(0).start()
    unit(0, 1)
    to_right(1).wait_recv()
    onward(1).start()
    unit(1, 0)
    to_left(0).wait_recv()
    to_left(1).wait_recv()
    unit(2, 0)
    to_left(2).wait_recv()
    onward(2).start()
    to_left(3).wait_recv()
    onward(3).start()
    sum_direct(1, 0).start()
    sum_direct(1, 1).start()
    unit(2, 1)
    sum_direct(2, 2).start()
    sum_direct(2, 3).start()
    to_right(2).wait_recv()
    to_right(3).wait_recv()
    unit(1, 1)
    onward(0).wait_recv()
    onward(1).wait_recv()
    unit(3, 0)
    sum_relay(0).start()
    sum_relay(1).start()
    onward(2).wait_recv()
    onward(3).wait_recv()
    unit(3, 1)
    sum_relay(2).start()
    sum_relay(3).start()
    for g in (0, 2, 1, 3):
        slot = 2 if g < 2 else 1
        sum_relay(g).wait_recv()
        partial[slot, group(g)] = (
            partial[slot, group(g)].astype(jnp.float32)
            + relayed[group(g)].astype(jnp.float32)
        ).astype(jnp.bfloat16)
        sum_direct(slot, g).start()

    def back(o):
        return pltpu.make_async_remote_copy(
            src_ref=partial.at[0, pl.ds(3 * o, 3)],
            dst_ref=out.at[pl.ds(3 * sp, 3)],
            send_sem=back_send.at[o],
            recv_sem=back_recv.at[o],
            device_id=(behind(o), dp),
            device_id_type=MESH,
        )

    def start_back(o, carry):
        back(o).start()
        return carry

    own_back = pltpu.make_async_copy(
        partial.at[0, pl.ds(0, 3)], out.at[pl.ds(3 * sp, 3)], back_send.at[0]
    )
    for g in (0, 2, 1, 3):
        sum_direct(2, g).wait_recv()
        sum_direct(1, g).wait_recv()
        partial[0, group(g)] = (
            partial[0, group(g)].astype(jnp.float32)
            + summed[0, group(g)].astype(jnp.float32)
            + summed[1, group(g)].astype(jnp.float32)
        ).astype(jnp.bfloat16)
        if g == 0:
            own_back.start()
        lax.fori_loop(max(4 * g, 1), 4 * g + 4, start_back, 0)

    for g in range(4):
        to_right(g).wait_send()
        to_left(g).wait_send()
        onward(g).wait_send()
        sum_direct(1, g).wait_send()
        sum_direct(2, g).wait_send()
        sum_relay(g).wait_send()
    own_back.wait()

    def drain(o, carry):
        go(o).wait_send()
        back(o).wait_send()
        back(o).wait_recv()
        return carry

    lax.fori_loop(1, 16, drain, 0)


def run_experts(rows, gate_w, raise_w, lower_w):
    width = rows.shape[2]
    part = gate_w.shape[1]
    any_space = pl.BlockSpec(memory_space=pl.ANY)
    return pl.pallas_call(
        expert_kernel,
        out_shape=jax.ShapeDtypeStruct(rows.shape, jnp.bfloat16),
        in_specs=[any_space] * 4,
        out_specs=any_space,
        scratch_shapes=[
            pltpu.VMEM((4, 48, 8, width), jnp.bfloat16),
            pltpu.VMEM((4, 48, 8, width), jnp.bfloat16),
            pltpu.VMEM((48, 8, width), jnp.bfloat16),
            pltpu.VMEM((2, 48, 8, width), jnp.bfloat16),
            pltpu.VMEM((width, 2 * part), jnp.bfloat16),
            pltpu.VMEM((width, 2 * part), jnp.bfloat16),
            pltpu.VMEM((2 * part, width), jnp.bfloat16),
            pltpu.VMEM((192, 2 * part), jnp.bfloat16),
            pltpu.SemaphoreType.DMA((3,)),
            pltpu.SemaphoreType.DMA((3,)),
            pltpu.SemaphoreType.DMA((3,)),
            pltpu.SemaphoreType.DMA((16,)),
            pltpu.SemaphoreType.DMA((16,)),
            pltpu.SemaphoreType.DMA((3, 4)),
            pltpu.SemaphoreType.DMA((3, 4)),
            pltpu.SemaphoreType.DMA((3, 4)),
            pltpu.SemaphoreType.DMA((3, 4)),
            pltpu.SemaphoreType.DMA((16,)),
            pltpu.SemaphoreType.DMA((16,)),
        ],
        compiler_params=pltpu.CompilerParams(
            collective_id=0, has_side_effects=True, vmem_limit_bytes=60 * 1024 * 1024
        ),
        name="routed_experts",
    )(rows, gate_w, raise_w, lower_w)


def causal_conv(series, tap_weights, rim_rows):
    padded = jnp.concatenate([rim_rows, series], axis=0).astype(jnp.float32)
    length = series.shape[0]
    running = jnp.zeros(series.shape, jnp.float32)
    for tap_index in range(tap_weights.shape[0]):
        running = running + tap_weights[tap_index] * lax.slice_in_dim(
            padded, tap_index, tap_index + length, axis=0
        )
    return jax.nn.silu(running).astype(jnp.bfloat16)


def ssd_blocks(x_conv, b_conv, c_conv, increment_delta, fading_exponent, init_state, block_len):
    length, head_count, head_width = x_conv.shape
    state_width = b_conv.shape[2]
    block_count = length // block_len
    x_block = x_conv.reshape(block_count, block_len, head_count, head_width)
    b_block = b_conv.reshape(block_count, block_len, head_count, state_width)
    c_block = c_conv.reshape(block_count, block_len, head_count, state_width)
    cumulative = jnp.cumsum(
        jnp.transpose(fading_exponent.reshape(block_count, block_len, head_count), (0, 2, 1)),
        axis=2,
    )
    step_heads = jnp.transpose(
        increment_delta.reshape(block_count, block_len, head_count), (0, 2, 1)
    )
    causal = jnp.arange(block_len)[:, None] >= jnp.arange(block_len)[None, :]
    within = jnp.exp(
        jnp.where(causal, cumulative[:, :, :, None] - cumulative[:, :, None, :], -jnp.inf)
    )
    scores = jnp.einsum("cthn,cshn->chts", c_block, b_block, preferred_element_type=jnp.float32)
    mixing = (scores * within * step_heads[:, :, None, :]).astype(jnp.bfloat16)
    diag_out = jnp.einsum("chts,cshp->cthp", mixing, x_block, preferred_element_type=jnp.float32)
    tail_decay = jnp.exp(cumulative[:, :, -1:] - cumulative) * step_heads
    scaled = (
        x_block.astype(jnp.float32) * jnp.transpose(tail_decay, (0, 2, 1))[:, :, :, None]
    ).astype(jnp.bfloat16)
    block_state = jnp.einsum("cshp,cshn->chpn", scaled, b_block, preferred_element_type=jnp.float32)
    totals = cumulative[:, :, -1]
    through = jnp.cumsum(totals, axis=0)
    before = through - totals
    earlier = jnp.arange(block_count)[:, None] > jnp.arange(block_count)[None, :]
    carry_weight = jnp.exp(
        jnp.where(earlier[:, :, None], before[:, None, :] - through[None, :, :], -jnp.inf)
    )
    entering = (
        jnp.einsum("cjh,jhpn->chpn", carry_weight, block_state)
        + jnp.exp(before)[:, :, None, None] * init_state[None]
    )
    reach_decay = jnp.transpose(jnp.exp(cumulative), (0, 2, 1))
    carried_out = (
        jnp.einsum("cthn,chpn->cthp", c_block.astype(jnp.float32), entering)
        * reach_decay[:, :, :, None]
    )
    outcome = (diag_out + carried_out).reshape(length, head_count, head_width)
    final_state = (
        jnp.einsum("jh,jhpn->hpn", jnp.exp(through[-1][None, :] - through), block_state)
        + jnp.exp(through[-1])[:, None, None] * init_state
    )
    return (outcome, final_state, through[-1])


def per_device(
    skip_connection_stream,
    emitted_valve_unscaled,
    channel_source_mapped,
    hidden_source_mapped,
    probe_mapped_values,
    increment_premapped,
    extra_log_fading,
    channel_fading_speed,
    channel_source_kernel,
    hidden_source_kernel,
    probe_kernel_coefficients,
    cluster_scaling_factor,
    emitted_mapping_matrix,
    standardize_scaling,
    standardize_offset,
    chosen_specialist_ids,
    specialist_mixing_shares,
    specialist_gating_matrices,
    raising_matrices,
    lowering_matrices,
):
    sp_size = lax.axis_size("sp")
    sp_index = lax.axis_index("sp")
    tok_rows = skip_connection_stream.shape[1]
    model_width = skip_connection_stream.shape[2]
    inner_width = HEADS * HEAD_DIM
    per_group = HEADS // GROUPS
    paired = HEAD_DIM + 2 * STATE
    head_count = HEADS // sp_size
    first_head = sp_index * head_count
    x_heads = channel_source_mapped[0].reshape(tok_rows, HEADS, HEAD_DIM)
    b_heads = jnp.repeat(
        hidden_source_mapped[0].reshape(tok_rows, GROUPS, STATE), per_group, axis=1
    )
    c_heads = jnp.repeat(probe_mapped_values[0].reshape(tok_rows, GROUPS, STATE), per_group, axis=1)
    payload = jnp.concatenate([x_heads, b_heads, c_heads], axis=2)
    arrived = lax.all_to_all(payload, "sp", split_axis=1, concat_axis=0, tiled=True)
    taps_x = lax.dynamic_slice_in_dim(
        channel_source_kernel.reshape(KERNEL, HEADS, HEAD_DIM), first_head, head_count, 1
    )
    taps_b = lax.dynamic_slice_in_dim(
        jnp.repeat(hidden_source_kernel.reshape(KERNEL, GROUPS, STATE), per_group, axis=1),
        first_head,
        head_count,
        1,
    )
    taps_c = lax.dynamic_slice_in_dim(
        jnp.repeat(probe_kernel_coefficients.reshape(KERNEL, GROUPS, STATE), per_group, axis=1),
        first_head,
        head_count,
        1,
    )
    rim_rows = jnp.zeros((KERNEL - 1, head_count, paired), jnp.bfloat16)
    convolved = causal_conv(arrived, jnp.concatenate([taps_x, taps_b, taps_c], axis=2), rim_rows)
    increment_delta = jax.nn.softplus(increment_premapped[0])
    speeds_per_channel = lax.dynamic_slice_in_dim(channel_fading_speed, first_head, head_count, 0)
    fading_exponent = extra_log_fading[0] - speeds_per_channel[None, :] * increment_delta
    init_state = jnp.zeros((head_count, HEAD_DIM, STATE), jnp.float32)
    outcome, final_state, total_decay = ssd_blocks(
        convolved[:, :, :HEAD_DIM],
        convolved[:, :, HEAD_DIM : HEAD_DIM + STATE],
        convolved[:, :, HEAD_DIM + STATE :],
        increment_delta,
        fading_exponent,
        init_state,
        BLK,
    )
    returned_rows = lax.all_to_all(
        outcome.astype(jnp.bfloat16), "sp", split_axis=0, concat_axis=1, tiled=True
    )
    blending_outcome = returned_rows.reshape(tok_rows, inner_width)
    gated = blending_outcome.astype(jnp.float32) * jax.nn.silu(
        emitted_valve_unscaled[0].astype(jnp.float32)
    )
    grouped = gated.reshape(tok_rows, GROUPS, inner_width // GROUPS)
    grouped = grouped * lax.rsqrt(jnp.mean(grouped * grouped, axis=-1, keepdims=True) + rms_eps)
    group_normed = (
        grouped.reshape(tok_rows, inner_width) * cluster_scaling_factor[None, :]
    ).astype(jnp.bfloat16)
    pre_norm = skip_connection_stream[0].astype(jnp.float32) + jnp.dot(
        group_normed, emitted_mapping_matrix, preferred_element_type=jnp.float32
    )
    centre = jnp.mean(pre_norm, axis=-1, keepdims=True)
    variance = jnp.mean(jnp.square(pre_norm - centre), axis=-1, keepdims=True)
    normed = (
        (pre_norm - centre) * lax.rsqrt(variance + norm_eps) * standardize_scaling[None, :]
        + standardize_offset[None, :]
    ).astype(jnp.bfloat16)
    slot_cap = 3 * tok_rows // sp_size
    flat_ids = chosen_specialist_ids[0].reshape(-1)
    matched = (flat_ids[:, None] == jnp.arange(sp_size, dtype=jnp.int32)[None, :]).astype(jnp.int32)
    ranked = jnp.cumsum(matched, axis=0) - 1
    target = flat_ids * slot_cap + jnp.sum(matched * ranked, axis=1)
    placing = (jnp.arange(sp_size * slot_cap, dtype=jnp.int32)[:, None] == target[None, :]).astype(
        jnp.bfloat16
    )
    placing = jnp.sum(placing.reshape(sp_size * slot_cap, tok_rows, 2), axis=2)
    outgoing = (
        jnp.dot(placing, normed, preferred_element_type=jnp.float32)
        .astype(jnp.bfloat16)
        .reshape(sp_size, slot_cap, model_width)
    )

    answered = run_experts(
        outgoing.reshape(-1, 8, model_width),
        specialist_gating_matrices[0],
        raising_matrices[0],
        lowering_matrices[0],
    )
    picked = answered.reshape(sp_size * slot_cap, model_width)[target.reshape(tok_rows, 2)]
    routed_sum = jnp.sum(
        specialist_mixing_shares[0][:, :, None] * picked.astype(jnp.float32), axis=1
    )
    layer_out = (normed.astype(jnp.float32) + routed_sum).astype(jnp.bfloat16)
    return layer_out[None]


def solution(mesh):
    placed = (
        P("dp", "sp", None),
        P("dp", "sp", None),
        P("dp", "sp", None),
        P("dp", "sp", None),
        P("dp", "sp", None),
        P("dp", None, "sp"),
        P("dp", None, "sp"),
        P(),
        P(),
        P(),
        P(),
        P(),
        P(),
        P(),
        P(),
        P("dp", "sp", None),
        P("dp", "sp", None),
        P("sp", None, "dp"),
        P("sp", None, "dp"),
        P("sp", "dp", None),
    )
    return jax.shard_map(
        per_device, mesh=mesh, in_specs=placed, out_specs=P("dp", "sp", None), check_vma=False
    )
```

profile of v0, /device:TPU:0, one launch (start us, length us, event | category | flops | bytes accessed | tf_op | source)
XLA Modules:
  0.0 199.6 jit_solution(18362534316384680243)
XLA Ops:
  0.0 0.9 copy.99
  1.0 1.0 copy.100
  1.9 1.1 copy.98
  3.2 0.9 pad_maximum_fusion
  4.2 8.2 %all-to-all-start = ((bf16[128,16,192]{0,2,1:T(8,128)(2,1)}), bf16[128,16,192]{0,2,1:T(8,128)(2,1)S(1)}, u32[]{:S(2)}, u32[]{:S(2)}) async-start(bf16[128,16,192]{0,2,1:T(8,128)(2,1)} %pad_maximum_fusion), calls=%async_computation | async-start | bytes 1572864 | tf_op jit(solution)/shard_map/all_to_all | solution.py:406
  12.4 0.1 copy.120
  12.5 0.1 eq.44
  12.6 0.1 eq.40
  12.8 0.6 reduce-window.6
  13.4 0.2 slice_reduce_fusion
  13.7 0.1 reduce_sum.74
  13.8 0.1 reduce_sum.76
  14.3 0.6 dynamic_slice.15
  14.9 0.7 fusion.44
  15.5 0.3 reduce_window_sum.37
  15.9 0.2 fusion.46
  16.1 0.1 reduce.5
  16.4 0.1 reshape.517
  16.8 10.1 %all-to-all-done = bf16[128,16,192]{0,2,1:T(8,128)(2,1)S(1)} async-done(((bf16[128,16,192]{0,2,1:T(8,128)(2,1)}), bf16[128,16,192]{0,2,1:T(8,128)(2,1)S(1)}, u32[]{:S(2)}, u32[]{:S(2)}) %all-to-all-start) | async-done | bytes 786464 | tf_op jit(solution)/shard_map/all_to_all | solution.py:406
  26.9 0.1 copy_bitcast_fusion
  27.0 0.3 pad_convert_fusion
  27.3 1.5 multiply_convert_fusion
  29.0 0.3 fusion.30
  29.3 0.3 fusion.8
  29.6 0.2 fusion.9
  29.8 0.8 fusion.11
  30.7 0.3 copy.125
  30.9 0.3 reshape.526
  31.2 0.5 broadcast.224
  31.7 11.6 %reduce.10 = bf16[2048,64]{1,0:T(8,128)(2,1)S(1)} reduce(bf16[2048,1,64]{2,1,0:T(2,128)(2,1)S(1)} %reshape.526, bf16[]{:T(256)} %broadcast.224), dimensions={1}, to_apply=%reshape.526.reduce_sub_computation | reduce | bytes 524290 | tf_op jit(solution)/shard_map/convert_element_type | solution.py:438
  43.3 1.1 reshape.531
  44.4 3.7 %all-to-all-start.1 = ((bf16[16,2,4096]{2,1,0:T(2,128)(2,1)}), bf16[16,2,4096]{2,1,0:T(2,128)(2,1)S(1)}, u32[]{:S(2)}, u32[]{:S(2)}) async-start(bf16[16,2,4096]{2,1,0:T(2,128)(2,1)} %reshape.531), calls=%async_computation.1 | async-start | bytes 524288 | tf_op jit(solution)/shard_map/all_to_all | solution.py:437
  48.1 0.2 copy.116
  48.5 8.1 %all-to-all-done.1 = bf16[16,2,4096]{2,1,0:T(2,128)(2,1)S(1)} async-done(((bf16[16,2,4096]{2,1,0:T(2,128)(2,1)}), bf16[16,2,4096]{2,1,0:T(2,128)(2,1)S(1)}, u32[]{:S(2)}, u32[]{:S(2)}) %all-to-all-start.1) | async-done | bytes 262176 | tf_op jit(solution)/shard_map/all_to_all | solution.py:437
  56.6 0.6 reshape.532
  57.2 0.6 copy.114
  58.0 0.3 multiply_reduce_fusion.2
  58.4 0.2 copy.115
  58.6 0.2 fusion.17
  58.8 0.2 copy-done
  59.0 3.0 %fusion.56 = (f32[128]{0:T(128)S(1)}, f32[128,2048]{1,0:T(8,128)S(1)}) fusion(bf16[128,1024]{0,1:T(8,128)(2,1)S(1)} %fusion.17, bf16[1024,2048]{1,0:T(8,128)(2,1)} %param.32, bf16[1,128,2048]{2,1,0:T(8,128)(2,1)S(1)} %copy-done), kind=kOutput, calls=%fused_computation.109 | convolution fusion | flops 537657216 | bytes 6029824 | tf_op jit(solution)/shard_map/dot_general | solution.py:449
  62.1 0.3 multiply_reduce_fusion.1
  62.4 1.8 fusion.rows
  64.2 123.8 %routed_experts.1 = bf16[48,8,2048]{2,1,0:T(8,128)(2,1)} custom-call(bf16[48,8,2048]{2,1,0:T(8,128)(2,1)} %fusion.rows, bf16[2048,640]{1,0:T(8,128)(2,1)} %bitcast.162, bf16[2048,640]{1,0:T(8,128)(2,1)} %bitcast.163, bf16[640,2048]{1,0:T(8,128)(2,1)} %bitcast.164), custom_call_target="tpu_custom_call" | custom-call | tf_op jit(solution)/shard_map/routed_experts/pallas_call | solution.py:275
  188.0 4.9 %gather_fusion = bf16[256,2048]{1,0:T(8,128)(2,1)} fusion(bf16[384,2048]{1,0:T(8,128)(2,1)} %bitcast.160, s32[1024]{0:T(1024)S(1)} %pad_clamp_fusion), kind=kCustom, calls=%fused_computation | custom fusion | bytes 2098176 | tf_op jit(solution)/shard_map/gather | solution.py:479
  193.0 2.4 %reshape.524 = f32[128,2,2048]{2,1,0:T(2,128)S(1)} reshape(bf16[256,2048]{1,0:T(8,128)(2,1)} %gather_fusion) | data formatting | bytes 3145728 | tf_op jit(solution)/shard_map/convert_element_type | solution.py:481
  195.3 3.2 %multiply_reduce_fusion = f32[128,2048]{1,0:T(8,128)S(1)} fusion(f32[128,2,2048]{2,1,0:T(2,128)S(1)} %reshape.524, f32[128,2]{1,0:T(8,128)S(1)} %copy.119), kind=kLoop, calls=%fused_computation.4 | loop fusion | flops 786432 | bytes 3146752 | tf_op jit(solution)/shard_map/reduce_sum | solution.py:480
  198.5 1.1 fusion.15
  (63 shorter events, 1.6 us)
Async XLA Ops:
  3.2 9.2 %copy-start.10 = (s32[1,128,2]{1,2,0:T(2,128)S(1)}, s32[1,128,2]{1,2,0:T(2,128)}, u32[]{:S(2)}) copy-start(s32[1,128,2]{1,2,0:T(2,128)} %param.35) | copy-start | bytes 3076
  3.2 10.8 %copy-start.8 = (f32[4,256]{1,0:T(4,128)S(1)}, f32[4,256]{1,0:T(4,128)}, u32[]{:S(2)}) copy-start(f32[4,256]{1,0:T(4,128)} %param.29) | copy-start | bytes 12292
  3.2 10.9 %copy-start.9 = (f32[4,256]{1,0:T(4,128)S(1)}, f32[4,256]{1,0:T(4,128)}, u32[]{:S(2)}) copy-start(f32[4,256]{1,0:T(4,128)} %param.30) | copy-start | bytes 12292
  3.2 11.0 %copy-start.5 = (f32[4,1024]{1,0:T(4,128)S(1)}, f32[4,1024]{1,0:T(4,128)}, u32[]{:S(2)}) copy-start(f32[4,1024]{1,0:T(4,128)} %param.28) | copy-start | bytes 49156
  3.2 11.1 %copy-start.12 = (f32[16]{0:T(128)S(1)}, f32[16]{0:T(128)}, u32[]{:S(2)}) copy-start(f32[16]{0:T(128)} %param.27) | copy-start | bytes 196
  3.2 11.7 %copy-start.4 = (f32[1,2048,1]{1,2,0:T(1,128)S(1)}, f32[1,2048,1]{1,2,0:T(1,128)}, u32[]{:S(2)}) copy-start(f32[1,2048,1]{1,2,0:T(1,128)} %param.25) | copy-start | bytes 24580
  3.2 11.6 %copy-start.6 = (f32[1,2048,1]{1,2,0:T(1,128)S(1)}, f32[1,2048,1]{1,2,0:T(1,128)}, u32[]{:S(2)}) copy-start(f32[1,2048,1]{1,2,0:T(1,128)} %param.26) | copy-start | bytes 24580
  4.2 22.7 %all-to-all-start = ((bf16[128,16,192]{0,2,1:T(8,128)(2,1)}), bf16[128,16,192]{0,2,1:T(8,128)(2,1)S(1)}, u32[]{:S(2)}, u32[]{:S(2)}) async-start(bf16[128,16,192]{0,2,1:T(8,128)(2,1)} %pad_maximum_fusion), calls=%async_computation | async-start | bytes 1572864 | tf_op jit(solution)/shard_map/all_to_all | solution.py:406
  31.2 16.9 %copy-start.1 = (bf16[1,128,1024]{2,1,0:T(8,128)(2,1)S(1)}, bf16[1,128,1024]{2,1,0:T(8,128)(2,1)}, u32[]{:S(2)}) copy-start(bf16[1,128,1024]{2,1,0:T(8,128)(2,1)} %param.21) | copy-start | bytes 786436
  31.7 16.6 %copy-start.11 = (f32[1,128,2]{1,2,0:T(2,128)S(1)}, f32[1,128,2]{1,2,0:T(2,128)}, u32[]{:S(2)}) copy-start(f32[1,128,2]{1,2,0:T(2,128)} %param.36) | copy-start | bytes 3076
  44.4 12.2 %all-to-all-start.1 = ((bf16[16,2,4096]{2,1,0:T(2,128)(2,1)}), bf16[16,2,4096]{2,1,0:T(2,128)(2,1)S(1)}, u32[]{:S(2)}, u32[]{:S(2)}) async-start(bf16[16,2,4096]{2,1,0:T(2,128)(2,1)} %reshape.531), calls=%async_computation.1 | async-start | bytes 524288 | tf_op jit(solution)/shard_map/all_to_all | solution.py:437
  57.9 0.7 copy-start.7
  58.0 1.0 copy-start
  59.0 3.3 %copy-start.2 = (f32[2048]{0:T(1024)S(1)}, f32[2048]{0:T(1024)}, u32[]{:S(2)}) copy-start(f32[2048]{0:T(1024)} %param.34) | copy-start | bytes 24580
  59.0 3.3 %copy-start.3 = (f32[2048]{0:T(1024)S(1)}, f32[2048]{0:T(1024)}, u32[]{:S(2)}) copy-start(f32[2048]{0:T(1024)} %param.33) | copy-start | bytes 24580
where the time goes:
time: 201 us; the launch traced here: 200 us
  Pallas kernels  124 us (62%)
  other arithmetic  21.8 us (11%)
  waiting for transfers between devices  18.2 us (9%)
  local copies, waits for them, and re-layouts  17 us (8%)
  starting transfers between devices  11.9 us (6%)
  matrix products  6.46 us (3%)
    pallas_call x1, Pallas kernels, run_experts(): pl.pallas_call(expert_kernel, out_shape=jax.ShapeDtypeStruct(rows.shape,...  124 us
    convert_element_type x1, other arithmetic, per_device(): outcome.astype(jnp.bfloat16)  11.6 us
    all_to_all x1, waiting for transfers between devices, per_device(): lax.all_to_all(payload, 'sp', split_axis=1, concat_axis=0, tiled=True)  10.1 us
    all_to_all x1, starting transfers between devices, per_device(): lax.all_to_all(payload, 'sp', split_axis=1, concat_axis=0, tiled=True)  8.16 us
    all_to_all x1, waiting for transfers between devices, per_device(): lax.all_to_all(outcome.astype(jnp.bfloat16), 'sp', split_axis=0, concat_a...  8.1 us
    unnamed x38, local copies, waits for them, and re-layouts  5.61 us
    gather x1, local copies, waits for them, and re-layouts, per_device(): answered.reshape(sp_size * slot_cap, model_width)  4.94 us
  transfers between devices with their start and end apart: 2, of which 2 were waited for; matrix products, arithmetic and copies ran while one was open for 2% of the time, Pallas kernels for 0%

commit v1 on v0

v1 whole, which is shorter than its diff:
```python
import jax
import jax.numpy as jnp
from jax import lax
from jax.experimental import pallas as pl
from jax.experimental.pallas import tpu as pltpu
from jax.sharding import PartitionSpec as P

MESH = pl.DeviceIdType.MESH
HEADS = 16
HEAD_DIM = 64
TOK = 128
INNER = 1024
SLOTS = 24
rms_eps = 1e-06
norm_eps = 1e-05
BF16 = jnp.bfloat16
F32 = jnp.float32
EXACT = lax.Precision.HIGHEST


def dot(a, b, precision=None):
    return jnp.dot(a, b, preferred_element_type=F32, precision=precision)


def dot_nt(a, b, precision=None):
    return lax.dot_general(
        a, b, (((1,), (1,)), ((), ())), preferred_element_type=F32, precision=precision
    )


def iota(shape, dim):
    return lax.broadcasted_iota(jnp.int32, shape, dim)


def layer_kernel(
    speed, skip, valve, chan, hid, probe, step_in, fade_in, tap_x, tap_b, tap_c, group_gain, out_w,
    gain, offset, ids, shares, gate_w, raise_w, lower_w,
    result,
    joined, steps, fades, conv, state, decay, state_in, decay_in, entering, entered, inside, out_v,
    pre, normed, placing, weighing, outgoing, answers,
    gathered, partial, relayed, summed, gate_v, raise_v, lower_v, hidden,
    load_sem, rim_send, rim_recv, step_send, step_recv, state_send, state_recv,
    enter_send, enter_recv,
    weight_sem, weight_send, weight_recv, go_send, go_recv, ring_send, ring_recv,
    sum_send, sum_recv, back_send, back_recv,
):
    sp = lax.axis_index("sp")
    dp = lax.axis_index("dp")
    z, y = lax.div(sp, 4), lax.rem(sp, 4)
    x, core = lax.div(dp, 2), lax.rem(dp, 2)
    right = (sp, lax.rem(x + 1, 4) * 2 + core)
    left = (sp, lax.rem(x + 3, 4) * 2 + core)
    twin = (sp, x * 2 + 1 - core)
    width = skip.shape[1]
    part = gate_w.shape[1]

    def ahead(o):
        return lax.rem(z + lax.div(o, 4), 4) * 4 + lax.rem(y + lax.rem(o, 4), 4)

    def behind(o):
        return lax.rem(z + 4 - lax.div(o, 4), 4) * 4 + lax.rem(y + 4 - lax.rem(o, 4), 4)

    def each(low, high, work):
        def step(o, carry):
            work(o)
            return carry

        lax.fori_loop(low, high, step, 0)

    barrier = pltpu.get_barrier_semaphore()
    each(
        1, 16,
        lambda o: pl.semaphore_signal(
            barrier, inc=1, device_id=(ahead(o), dp), device_id_type=MESH
        ),
    )
    for friend in (left, right, twin):
        pl.semaphore_signal(barrier, inc=1, device_id=friend, device_id_type=MESH)

    spans = ((chan, 0, INNER), (hid, INNER, 256), (probe, INNER + 256, 256))
    own_loads = [
        pltpu.make_async_copy(
            ref, joined.at[pl.ds(1, 16), :, pl.ds(low, size)], load_sem.at[k]
        )
        for k, (ref, low, size) in enumerate(spans)
    ]
    own_loads.append(
        pltpu.make_async_copy(step_in.at[sp], steps.at[sp], load_sem.at[3])
    )
    own_loads.append(
        pltpu.make_async_copy(fade_in.at[sp], fades.at[sp], load_sem.at[4])
    )
    out_load = pltpu.make_async_copy(out_w, out_v, load_sem.at[5])
    for copy in own_loads:
        copy.start()
    loads, gifts = [], []
    for k, (source, target) in enumerate(
        ((gate_w, gate_v), (raise_w, raise_v), (lower_w, lower_v))
    ):
        if k < 2:
            mine, theirs = target.at[:, pl.ds(0, part)], target.at[:, pl.ds(part, part)]
        else:
            mine, theirs = target.at[pl.ds(0, part)], target.at[pl.ds(part, part)]
        loads.append(pltpu.make_async_copy(source, mine, weight_sem.at[k]))
        gifts.append(
            pltpu.make_async_remote_copy(
                src_ref=source,
                dst_ref=theirs,
                send_sem=weight_send.at[k],
                recv_sem=weight_recv.at[k],
                device_id=twin,
                device_id_type=MESH,
            )
        )

    pl.semaphore_wait(barrier, 18)

    def step_copy(o, source, target, which):
        return pltpu.make_async_remote_copy(
            src_ref=source.at[ahead(o)],
            dst_ref=target.at[sp],
            send_sem=step_send.at[which, o],
            recv_sem=step_recv.at[which, o],
            device_id=(ahead(o), dp),
            device_id_type=MESH,
        )

    def send_steps(o):
        step_copy(o, step_in, steps, 0).start()
        step_copy(o, fade_in, fades, 1).start()

    each(1, 16, send_steps)
    rims = [
        pltpu.make_async_remote_copy(
            src_ref=ref.at[pl.ds(15, 1)],
            dst_ref=joined.at[pl.ds(0, 1), :, pl.ds(low, size)],
            send_sem=rim_send.at[k],
            recv_sem=rim_recv.at[k],
            device_id=(lax.rem(sp + 1, 16), dp),
            device_id_type=MESH,
        )
        for k, (ref, low, size) in enumerate(spans)
    ]
    for copy in rims:
        copy.start()
    out_load.start()
    for copy in loads + gifts:
        copy.start()
    for copy in own_loads:
        copy.wait()
    for copy in rims:
        copy.wait_recv()

    def convolve(cols, taps):
        block = joined[:, :, cols].reshape(TOK + 8, 256).astype(F32)
        block = jnp.where(iota((TOK + 8, 256), 0) + 8 * sp >= 8, block, 0.0)
        running = taps[0:1] * block[5 : 5 + TOK]
        for k in range(1, 4):
            running = running + taps[k : k + 1] * block[5 + k : 5 + k + TOK]
        conv[:, cols] = jax.nn.silu(running).astype(BF16)

    def convolve_x(k):
        cols = pl.ds(pl.multiple_of(k * 256, 256), 256)
        convolve(cols, tap_x[:, cols])

    each(0, 4, convolve_x)
    convolve(pl.ds(INNER, 256), tap_b[...])
    convolve(pl.ds(INNER + 256, 256), tap_c[...])

    def wait_steps(o):
        step_copy(o, step_in, steps, 0).wait_recv()
        step_copy(o, fade_in, fades, 1).wait_recv()

    each(1, 16, wait_steps)
    row = iota((HEADS, TOK), 0)
    speeds = jnp.zeros((HEADS, TOK), F32)
    for h in range(HEADS):
        speeds = jnp.where(row == h, speed[h], speeds)
    raw = steps[...].reshape(HEADS, TOK)
    step = jnp.maximum(raw, 0.0) + jnp.log1p(jnp.exp(-jnp.abs(raw)))
    fading = fades[...].reshape(HEADS, TOK) - speeds * step
    later = iota((TOK, TOK), 0)
    sooner = iota((TOK, TOK), 1)
    causal = later >= sooner
    triangle = causal.astype(F32)
    cum_row = dot_nt(fading, triangle, EXACT)
    cum_col = dot_nt(triangle, fading, EXACT)
    step_col = dot_nt((later == sooner).astype(F32), step, EXACT)
    spread = (lax.div(iota((HEADS, INNER), 1), HEAD_DIM) == iota((HEADS, INNER), 0)).astype(F32)
    last = cum_col[TOK - 1 : TOK]
    tail_wide = dot(jnp.exp(last - cum_col) * step_col, spread, EXACT)
    decay_wide = dot(jnp.broadcast_to(jnp.exp(last), (8, HEADS)), spread, EXACT)
    for k in range(2):
        decay[k] = decay_wide[0:1, 512 * k : 512 * k + 512]
    scaled = (conv[:, 0:INNER].astype(F32) * tail_wide).astype(BF16)
    for q in range(2):
        b_pair = conv[:, INNER + 128 * q : INNER + 128 * q + 128]
        both = dot(b_pair.T, scaled[:, 512 * q : 512 * q + 512])
        state[:, 512 * q : 512 * q + 256] = both[0:64, 0:256]
        state[:, 512 * q + 256 : 512 * q + 512] = both[64:128, 256:512]

    def place_of(k):
        return (
            pl.ds(pl.multiple_of(lax.div(k, 2) * 8, 8), 8),
            pl.ds(pl.multiple_of(lax.rem(k, 2) * 512, 512), 512),
        )

    def state_copy(o):
        rows, cols = place_of(ahead(o))
        return pltpu.make_async_remote_copy(
            src_ref=state.at[rows, cols],
            dst_ref=state_in.at[sp],
            send_sem=state_send.at[0, o],
            recv_sem=state_recv.at[0, o],
            device_id=(ahead(o), dp),
            device_id_type=MESH,
        )

    def decay_copy(o):
        return pltpu.make_async_remote_copy(
            src_ref=decay.at[lax.rem(ahead(o), 2)],
            dst_ref=decay_in.at[sp],
            send_sem=state_send.at[1, o],
            recv_sem=state_recv.at[1, o],
            device_id=(ahead(o), dp),
            device_id_type=MESH,
        )

    def send_state(o):
        decay_copy(o).start()
        state_copy(o).start()

    each(1, 16, send_state)
    my_rows, my_cols = place_of(sp)
    state_in[sp] = state[my_rows, my_cols]
    decay_in[sp] = decay[lax.rem(sp, 2)]

    low_half = iota((TOK, TOK), 1) < 64
    for q in range(2):
        b_pair = conv[:, INNER + 128 * q : INNER + 128 * q + 128]
        c_pair = conv[:, INNER + 256 + 128 * q : INNER + 256 + 128 * q + 128]
        for g in range(2):
            c_one = jnp.where(low_half == (g == 0), c_pair, jnp.zeros_like(c_pair))
            scores = dot_nt(c_one, b_pair)
            for i in range(2):
                first = 8 * q + 4 * g + 2 * i
                x_pair = conv[:, 64 * first : 64 * first + 128]
                total = None
                for h in (first, first + 1):
                    gap = jnp.where(
                        causal, cum_col[:, h : h + 1] - cum_row[h : h + 1, :], -1e30
                    )
                    mixing = (scores * jnp.exp(gap) * step[h : h + 1, :]).astype(BF16)
                    x_one = jnp.where(low_half == (h == first), x_pair, jnp.zeros_like(x_pair))
                    term = dot(mixing, x_one)
                    total = term if total is None else total + term
                inside[:, 64 * first : 64 * first + 128] = total

    def placing_rows():
        expert = iota((16, TOK), 0)
        first, second = expert == ids[0:1, :], expert == ids[1:2, :]
        named = first | second
        share = jnp.where(first, shares[0:1, :], 0.0) + jnp.where(second, shares[1:2, :], 0.0)
        before = (later < sooner).astype(BF16)
        rank = dot(named.astype(F32).astype(BF16), before)
        rank = jnp.where(named, rank, -1.0)
        slot = iota((SLOTS, TOK), 0).astype(F32)
        chosen = jnp.concatenate(
            [(rank[e : e + 1, :] == slot).astype(F32) for e in range(16)], axis=0
        )
        weights = jnp.concatenate(
            [
                jnp.where(rank[e : e + 1, :] == slot, share[e : e + 1, :], 0.0)
                for e in range(16)
            ],
            axis=0,
        )
        placing[...] = chosen.astype(BF16)
        rest = weights.T
        for k in range(3):
            piece = rest.astype(BF16)
            weighing[pl.ds(TOK * k, TOK), :] = piece
            rest = rest - piece.astype(F32)

    placing_rows()

    def wait_state(o):
        decay_copy(o).wait_recv()
        state_copy(o).wait_recv()

    each(1, 16, wait_state)

    def advance(j, held):
        entering[j] = held
        return decay_in[j] * held + state_in[j]

    lax.fori_loop(0, 16, advance, jnp.zeros((8, 512), F32))

    def enter_copy(o):
        rows, cols = place_of(sp)
        return pltpu.make_async_remote_copy(
            src_ref=entering.at[ahead(o)],
            dst_ref=entered.at[rows, cols],
            send_sem=enter_send.at[o],
            recv_sem=enter_recv.at[o],
            device_id=(ahead(o), dp),
            device_id_type=MESH,
        )

    each(1, 16, lambda o: enter_copy(o).start())
    entered[my_rows, my_cols] = entering[sp]
    reach_wide = dot(jnp.exp(cum_col), spread, EXACT)
    each(1, 16, lambda o: enter_copy(o).wait_recv())

    nothing = jnp.zeros((64, 256), F32)
    blocks = []
    for q in range(2):
        c_pair = conv[:, INNER + 256 + 128 * q : INNER + 256 + 128 * q + 128]
        low, high = entered[:, 512 * q : 512 * q + 256], entered[:, 512 * q + 256 : 512 * q + 512]
        both = jnp.concatenate(
            [
                jnp.concatenate([low, nothing], axis=1),
                jnp.concatenate([nothing, high], axis=1),
            ],
            axis=0,
        )
        carried = dot(c_pair.astype(F32), both, EXACT)
        for g in range(2):
            low_col = 512 * q + 256 * g
            mixed = (
                inside[:, low_col : low_col + 256]
                + reach_wide[:, low_col : low_col + 256] * carried[:, 256 * g : 256 * g + 256]
            ).astype(BF16)
            gated = mixed.astype(F32) * jax.nn.silu(valve[:, low_col : low_col + 256].astype(F32))
            level = lax.rsqrt(jnp.mean(gated * gated, axis=1, keepdims=True) + rms_eps)
            blocks.append(
                (gated * level * group_gain[:, low_col : low_col + 256]).astype(BF16)
            )
    group_normed = jnp.concatenate(blocks, axis=1)
    out_load.wait()

    def project(k):
        cols = pl.ds(pl.multiple_of(k * 256, 256), 256)
        pre[:, cols] = skip[:, cols].astype(F32) + dot(group_normed, out_v[:, cols])

    each(0, width // 256, project)

    def standardize(k):
        rows = pl.ds(pl.multiple_of(k * 16, 16), 16)
        block = pre[rows, :]
        shifted = block - jnp.mean(block, axis=1, keepdims=True)
        level = lax.rsqrt(jnp.mean(shifted * shifted, axis=1, keepdims=True) + norm_eps)
        normed[rows, :] = (shifted * level * gain[...] + offset[...]).astype(BF16)

    each(0, TOK // 16, standardize)
    flat_outgoing = outgoing.reshape(16 * SLOTS, width)

    def route(k):
        cols = pl.ds(pl.multiple_of(k * 256, 256), 256)
        flat_outgoing[:, cols] = dot(placing[...], normed[:, cols]).astype(BF16)

    each(0, width // 256, route)

    def go(o):
        return pltpu.make_async_remote_copy(
            src_ref=outgoing.at[pl.ds(3 * ahead(o), 3)],
            dst_ref=gathered.at[0, pl.ds(3 * o, 3)],
            send_sem=go_send.at[o],
            recv_sem=go_recv.at[o],
            device_id=(ahead(o), dp),
            device_id_type=MESH,
        )

    each(1, 16, lambda o: go(o).start())
    gathered[0, 0:3] = outgoing[pl.ds(3 * sp, 3)]

    def group(g):
        return pl.ds(12 * g, 12)

    def ring(src_slot, dst_slot, g, target, lane):
        return pltpu.make_async_remote_copy(
            src_ref=gathered.at[src_slot, group(g)],
            dst_ref=gathered.at[dst_slot, group(g)],
            send_sem=ring_send.at[lane, g],
            recv_sem=ring_recv.at[dst_slot - 1, g],
            device_id=target,
            device_id_type=MESH,
        )

    def to_right(g):
        return ring(0, 1, g, right, 0)

    def to_left(g):
        return ring(0, 2, g, left, 1)

    def onward(g):
        return ring(1, 3, g, right, 2) if g < 2 else ring(2, 3, g, left, 2)

    for g in range(4):
        each(max(4 * g, 1), 4 * g + 4, lambda o: go(o).wait_recv())
        to_right(g).start()
        to_left(g).start()

    for copy in loads:
        copy.wait()
    for copy in gifts:
        copy.wait()

    tile = 256

    def unit(slot, half):
        rows_here = gathered.at[slot, pl.ds(24 * half, 24)].reshape(192, width)
        block = rows_here[...]

        def up(k):
            cols = pl.ds(pl.multiple_of(k * tile, tile), tile)
            gate_val = jnp.dot(block, gate_v[:, cols], preferred_element_type=F32)
            up_val = jnp.dot(block, raise_v[:, cols], preferred_element_type=F32)
            hidden[:, cols] = (jax.nn.silu(gate_val) * up_val).astype(BF16)

        each(0, 2 * part // tile, up)
        target = partial.at[slot, pl.ds(24 * half, 24)].reshape(192, width)

        def down(k):
            cols = pl.ds(pl.multiple_of(k * tile, tile), tile)
            target[:, cols] = jnp.dot(
                hidden[...], lower_v[:, cols], preferred_element_type=F32
            ).astype(BF16)

        each(0, width // tile, down)

    def sum_direct(slot, g):
        side = 0 if slot == 2 else 1
        return pltpu.make_async_remote_copy(
            src_ref=partial.at[slot, group(g)],
            dst_ref=summed.at[side, group(g)],
            send_sem=sum_send.at[side, g],
            recv_sem=sum_recv.at[side, g],
            device_id=right if slot == 2 else left,
            device_id_type=MESH,
        )

    def sum_relay(g):
        return pltpu.make_async_remote_copy(
            src_ref=partial.at[3, group(g)],
            dst_ref=relayed.at[group(g)],
            send_sem=sum_send.at[2, g],
            recv_sem=sum_recv.at[2, g],
            device_id=right if g < 2 else left,
            device_id_type=MESH,
        )

    unit(0, 0)
    to_right(0).wait_recv()
    onward(0).start()
    unit(0, 1)
    to_right(1).wait_recv()
    onward(1).start()
    unit(1, 0)
    to_left(0).wait_recv()
    to_left(1).wait_recv()
    unit(2, 0)
    to_left(2).wait_recv()
    onward(2).start()
    to_left(3).wait_recv()
    onward(3).start()
    sum_direct(1, 0).start()
    sum_direct(1, 1).start()
    unit(2, 1)
    sum_direct(2, 2).start()
    sum_direct(2, 3).start()
    to_right(2).wait_recv()
    to_right(3).wait_recv()
    unit(1, 1)
    onward(0).wait_recv()
    onward(1).wait_recv()
    unit(3, 0)
    sum_relay(0).start()
    sum_relay(1).start()
    onward(2).wait_recv()
    onward(3).wait_recv()
    unit(3, 1)
    sum_relay(2).start()
    sum_relay(3).start()
    for g in (0, 2, 1, 3):
        slot = 2 if g < 2 else 1
        sum_relay(g).wait_recv()
        partial[slot, group(g)] = (
            partial[slot, group(g)].astype(F32)
            + relayed[group(g)].astype(F32)
        ).astype(BF16)
        sum_direct(slot, g).start()

    def back(o):
        return pltpu.make_async_remote_copy(
            src_ref=partial.at[0, pl.ds(3 * o, 3)],
            dst_ref=answers.at[pl.ds(3 * sp, 3)],
            send_sem=back_send.at[o],
            recv_sem=back_recv.at[o],
            device_id=(behind(o), dp),
            device_id_type=MESH,
        )

    for g in (0, 2, 1, 3):
        sum_direct(2, g).wait_recv()
        sum_direct(1, g).wait_recv()
        partial[0, group(g)] = (
            partial[0, group(g)].astype(F32)
            + summed[0, group(g)].astype(F32)
            + summed[1, group(g)].astype(F32)
        ).astype(BF16)
        each(max(4 * g, 1), 4 * g + 4, lambda o: back(o).start())
        if g == 0:
            answers[pl.ds(3 * sp, 3)] = partial[0, 0:3]

    for copy in rims:
        copy.wait_send()
    for g in range(4):
        to_right(g).wait_send()
        to_left(g).wait_send()
        onward(g).wait_send()
        sum_direct(1, g).wait_send()
        sum_direct(2, g).wait_send()
        sum_relay(g).wait_send()

    def drain(o):
        step_copy(o, step_in, steps, 0).wait_send()
        step_copy(o, fade_in, fades, 1).wait_send()
        decay_copy(o).wait_send()
        state_copy(o).wait_send()
        enter_copy(o).wait_send()
        go(o).wait_send()
        back(o).wait_send()
        back(o).wait_recv()

    each(1, 16, drain)
    flat_answers = answers.reshape(16 * SLOTS, width)

    def finish(k):
        cols = pl.ds(pl.multiple_of(k * 256, 256), 256)
        terms = dot(weighing[...], flat_answers[:, cols])
        routed = terms[0:TOK] + terms[TOK : 2 * TOK] + terms[2 * TOK : 3 * TOK]
        result[:, cols] = (normed[:, cols].astype(F32) + routed).astype(BF16)

    each(0, width // 256, finish)


def per_device(
    skip_connection_stream,
    emitted_valve_unscaled,
    channel_source_mapped,
    hidden_source_mapped,
    probe_mapped_values,
    increment_premapped,
    extra_log_fading,
    channel_fading_speed,
    channel_source_kernel,
    hidden_source_kernel,
    probe_kernel_coefficients,
    cluster_scaling_factor,
    emitted_mapping_matrix,
    standardize_scaling,
    standardize_offset,
    chosen_specialist_ids,
    specialist_mixing_shares,
    specialist_gating_matrices,
    raising_matrices,
    lowering_matrices,
):
    width = skip_connection_stream.shape[2]
    part = specialist_gating_matrices.shape[2]
    far = pl.BlockSpec(memory_space=pl.ANY)
    near = pl.BlockSpec(memory_space=pltpu.VMEM)
    scalars = pl.BlockSpec(memory_space=pltpu.SMEM)
    dma = pltpu.SemaphoreType.DMA
    rows = 2 * SLOTS
    out = pl.pallas_call(
        layer_kernel,
        out_shape=jax.ShapeDtypeStruct((TOK, width), BF16),
        in_specs=[scalars, near, near] + [far] * 5 + [near] * 4 + [far] + [near] * 4 + [far] * 3,
        out_specs=near,
        scratch_shapes=[
            pltpu.VMEM((17, 8, 1536), BF16),
            pltpu.VMEM((HEADS, 1, TOK), F32),
            pltpu.VMEM((HEADS, 1, TOK), F32),
            pltpu.VMEM((TOK, 1536), BF16),
            pltpu.VMEM((64, INNER), F32),
            pltpu.VMEM((2, 1, 512), F32),
            pltpu.VMEM((16, 8, 512), F32),
            pltpu.VMEM((16, 1, 512), F32),
            pltpu.VMEM((16, 8, 512), F32),
            pltpu.VMEM((64, INNER), F32),
            pltpu.VMEM((TOK, INNER), F32),
            pltpu.VMEM((INNER, width), BF16),
            pltpu.VMEM((TOK, width), F32),
            pltpu.VMEM((TOK, width), BF16),
            pltpu.VMEM((16 * SLOTS, TOK), BF16),
            pltpu.VMEM((3 * TOK, 16 * SLOTS), BF16),
            pltpu.VMEM((rows, 8, width), BF16),
            pltpu.VMEM((rows, 8, width), BF16),
            pltpu.VMEM((4, rows, 8, width), BF16),
            pltpu.VMEM((4, rows, 8, width), BF16),
            pltpu.VMEM((rows, 8, width), BF16),
            pltpu.VMEM((2, rows, 8, width), BF16),
            pltpu.VMEM((width, 2 * part), BF16),
            pltpu.VMEM((width, 2 * part), BF16),
            pltpu.VMEM((2 * part, width), BF16),
            pltpu.VMEM((192, 2 * part), BF16),
            dma((6,)), dma((3,)), dma((3,)), dma((2, 16)), dma((2, 16)), dma((2, 16)), dma((2, 16)),
            dma((16,)), dma((16,)), dma((3,)), dma((3,)), dma((3,)), dma((16,)), dma((16,)),
            dma((3, 4)), dma((3, 4)), dma((3, 4)), dma((3, 4)), dma((16,)), dma((16,)),
        ],
        compiler_params=pltpu.CompilerParams(
            collective_id=0, has_side_effects=True, vmem_limit_bytes=62 * 1024 * 1024
        ),
        name="layer",
    )(
        channel_fading_speed,
        skip_connection_stream[0],
        emitted_valve_unscaled[0],
        channel_source_mapped.reshape(16, 8, INNER),
        hidden_source_mapped.reshape(16, 8, 256),
        probe_mapped_values.reshape(16, 8, 256),
        increment_premapped.reshape(16, 1, TOK),
        extra_log_fading.reshape(16, 1, TOK),
        channel_source_kernel,
        hidden_source_kernel,
        probe_kernel_coefficients,
        cluster_scaling_factor[None, :],
        emitted_mapping_matrix,
        standardize_scaling[None, :],
        standardize_offset[None, :],
        chosen_specialist_ids[0].T,
        specialist_mixing_shares[0].T,
        specialist_gating_matrices[0],
        raising_matrices[0],
        lowering_matrices[0],
    )
    return out[None]


def solution(mesh):
    placed = (
        P("dp", "sp", None),
        P("dp", "sp", None),
        P("dp", "sp", None),
        P("dp", "sp", None),
        P("dp", "sp", None),
        P("dp", None, "sp"),
        P("dp", None, "sp"),
        P(),
        P(),
        P(),
        P(),
        P(),
        P(),
        P(),
        P(),
        P("dp", "sp", None),
        P("dp", "sp", None),
        P("sp", None, "dp"),
        P("sp", None, "dp"),
        P("sp", "dp", None),
    )
    return jax.shard_map(
        per_device, mesh=mesh, in_specs=placed, out_specs=P("dp", "sp", None), check_vma=False
    )
```

time: 201 us -> 157 us (0.78)
  Pallas kernels: 124 us -> 155 us
  other arithmetic: 21.8 us -> 0 us
  waiting for transfers between devices: 18.2 us -> 0 us
  local copies, waits for them, and re-layouts: 17 us -> 1.88 us
  starting transfers between devices: 11.9 us -> 0 us
  matrix products: 6.46 us -> 0 us
    pallas_call x1, Pallas kernels: 124 us -> 155 us  [per_device(): pl.pallas_call(layer_kernel, out_shape=jax.ShapeDtypeStruct((TOK, width),...]
    all_to_all x2 -> x0, waiting for transfers between devices: 18.2 us -> none  [the longest x1 10.1 us: per_device(): lax.all_to_all(payload, 'sp', split_axis=1, concat_axis=0, tiled=True)]
    convert_element_type x7 -> x0, other arithmetic: 13.6 us -> none  [the longest x1 11.6 us: per_device(): outcome.astype(jnp.bfloat16)]
    all_to_all x2 -> x0, starting transfers between devices: 11.9 us -> none  [the longest x1 8.16 us: per_device(): lax.all_to_all(payload, 'sp', split_axis=1, concat_axis=0, tiled=True)]
    dot_general x6 -> x0, matrix products: 6.46 us -> none  [the longest x1 3.03 us: per_device(): jnp.dot(group_normed, emitted_mapping_matrix, preferred_element_type=jnp....]
    gather x1 -> x0, local copies, waits for them, and re-layouts: 4.94 us -> none  [per_device(): answered.reshape(sp_size * slot_cap, model_width)]
    reduce_sum x6 -> x0, other arithmetic: 3.95 us -> none  [the longest x1 3.16 us: per_device(): jnp.sum(specialist_mixing_shares[0][:, :, None] * picked.astype(jnp.float...]
    unnamed x38 -> x1, local copies, waits for them, and re-layouts: 5.61 us -> 1.88 us
  transfers between devices with their start and end apart: 2 -> 0, of which waited for: 2 -> 0; matrix products, arithmetic and copies ran while one was open for 2% -> 0% of each run, Pallas kernels for 0% -> 0%
where the time goes in v1:
time: 157 us
  Pallas kernels  155 us (99%)
  local copies, waits for them, and re-layouts  1.88 us (1%)
    pallas_call x1, Pallas kernels, per_device(): pl.pallas_call(layer_kernel, out_shape=jax.ShapeDtypeStruct((TOK, width),...  155 us

profile of v1, /device:TPU:0, one launch (start us, length us, event | category | flops | bytes accessed | tf_op | source)
XLA Modules:
  0.0 156.6 jit_solution(8205639262988134992)
XLA Ops:
  0.0 154.7 %layer.1 = bf16[128,2048]{1,0:T(8,128)(2,1)} custom-call(f32[16]{0:T(128)} %speed.1, bf16[128,2048]{1,0:T(8,128)(2,1)} %bitcast.24, bf16[128,1024]{1,0:T(8,128)(2,1)} %bitcast.25, bf16[16,8,1024]{2,1,0:T(8,128)(2,1)} %bitcast.26, bf16[16,8,256]{2,1,0:T(8,128)(2,1)} %bitcast.27, bf16[16,8,256]{2,1,0:T(8,128)(2,1)} %bitcast.28, f32[16,1,128]{2,1,0:T(1,128)} %bitcast.29, ...), custom_call_target="tpu_custom_call" | custom-call | tf_op jit(solution)/shard_map/layer/pallas_call | solution.py:577
  154.7 1.9 %copy.22 = bf16[1,128,2048]{2,1,0:T(8,128)(2,1)} copy(bf16[1,128,2048]{2,1,0:T(8,128)(2,1)} %bitcast.23) | data formatting | bytes 1048576

commit v2 on v1

--- a/solution.py
+++ b/solution.py
@@ -11,6 +11,7 @@
 TOK = 128
 INNER = 1024
 SLOTS = 24
+NEAR = 1280
 rms_eps = 1e-06
 norm_eps = 1e-05
 BF16 = jnp.bfloat16
@@ -36,13 +37,15 @@
     speed, skip, valve, chan, hid, probe, step_in, fade_in, tap_x, tap_b, tap_c, group_gain, out_w,
     gain, offset, ids, shares, gate_w, raise_w, lower_w,
     result,
-    joined, steps, fades, conv, state, decay, state_in, decay_in, entering, entered, inside, out_v,
-    pre, normed, placing, weighing, outgoing, answers,
+    joined, rim, steps, fades, names, parts, conv, state, decay, state_in, decay_in, entering,
+    entered, inside, out_v, pre, normed, placing, weighing, outgoing, answers,
+    tokens, far_rows, far_answers, token_sum, token_out, token_relay, token_in,
     gathered, partial, relayed, summed, gate_v, raise_v, lower_v, hidden,
-    load_sem, rim_send, rim_recv, step_send, step_recv, state_send, state_recv,
-    enter_send, enter_recv,
+    load_sem, rim_send, rim_recv, name_send, name_recv, step_send, step_recv,
+    state_send, state_recv, enter_send, enter_recv,
     weight_sem, weight_send, weight_recv, go_send, go_recv, ring_send, ring_recv,
-    sum_send, sum_recv, back_send, back_recv,
+    sum_send, sum_recv, back_send, back_recv, token_send, token_recv, far_send, far_recv,
+    home_send, home_recv, tsum_send, tsum_recv,
 ):
     sp = lax.axis_index("sp")
     dp = lax.axis_index("dp")
@@ -50,15 +53,18 @@
     x, core = lax.div(dp, 2), lax.rem(dp, 2)
     right = (sp, lax.rem(x + 1, 4) * 2 + core)
     left = (sp, lax.rem(x + 3, 4) * 2 + core)
+    across = (sp, lax.rem(x + 2, 4) * 2 + core)
     twin = (sp, x * 2 + 1 - core)
     width = skip.shape[1]
     part = gate_w.shape[1]
 
     def ahead(o):
-        return lax.rem(z + lax.div(o, 4), 4) * 4 + lax.rem(y + lax.rem(o, 4), 4)
+        i = lax.rem(o, 4)
+        return lax.rem(z + i, 4) * 4 + lax.rem(y + i + lax.div(o, 4), 4)
 
     def behind(o):
-        return lax.rem(z + 4 - lax.div(o, 4), 4) * 4 + lax.rem(y + 4 - lax.rem(o, 4), 4)
+        i = lax.rem(o, 4)
+        return lax.rem(z + 4 - i, 4) * 4 + lax.rem(y + 8 - i - lax.div(o, 4), 4)
 
     def each(low, high, work):
         def step(o, carry):
@@ -74,13 +80,13 @@
             barrier, inc=1, device_id=(ahead(o), dp), device_id_type=MESH
         ),
     )
-    for friend in (left, right, twin):
+    for friend in (left, right, across, twin):
         pl.semaphore_signal(barrier, inc=1, device_id=friend, device_id_type=MESH)
 
     spans = ((chan, 0, INNER), (hid, INNER, 256), (probe, INNER + 256, 256))
     own_loads = [
         pltpu.make_async_copy(
-            ref, joined.at[pl.ds(1, 16), :, pl.ds(low, size)], load_sem.at[k]
+            ref, joined.at[:, :, pl.ds(low, size)], load_sem.at[k]
         )
         for k, (ref, low, size) in enumerate(spans)
     ]
@@ -90,6 +96,8 @@
     own_loads.append(
         pltpu.make_async_copy(fade_in.at[sp], fades.at[sp], load_sem.at[4])
     )
+    own_loads.append(pltpu.make_async_copy(ids, names.at[0], load_sem.at[6]))
+    own_loads.append(pltpu.make_async_copy(shares, parts.at[0], load_sem.at[7]))
     out_load = pltpu.make_async_copy(out_w, out_v, load_sem.at[5])
     for copy in own_loads:
         copy.start()
@@ -113,7 +121,40 @@
             )
         )
 
-    pl.semaphore_wait(barrier, 18)
+    out_load.start()
+    for copy in loads:
+        copy.start()
+    for copy in own_loads:
+        copy.wait()
+
+    def filtered(block, taps):
+        high = block.shape[0] - 8
+        running = taps[0:1] * block[5 : 5 + high]
+        for k in range(1, 4):
+            running = running + taps[k : k + 1] * block[5 + k : 5 + k + high]
+        return jax.nn.silu(running).astype(BF16)
+
+    def convolve(cols, taps):
+        block = joined[:, :, cols].reshape(TOK, 256).astype(F32)
+        block = jnp.concatenate([jnp.zeros((8, 256), F32), block], axis=0)
+        conv[:, cols] = filtered(block, taps)
+
+    def convolve_rim(cols, taps):
+        before = rim[:, :, cols].reshape(8, 256).astype(F32) * (sp > 0).astype(F32)
+        block = joined[0:2, :, cols].reshape(16, 256).astype(F32)
+        conv[0:16, cols] = filtered(jnp.concatenate([before, block], axis=0), taps)
+
+    def begin(work):
+        def work_x(k):
+            cols = pl.ds(pl.multiple_of(k * 256, 256), 256)
+            work(cols, tap_x[:, cols])
+
+        each(0, 4, work_x)
+        work(pl.ds(INNER, 256), tap_b[...])
+        work(pl.ds(INNER + 256, 256), tap_c[...])
+
+    begin(convolve)
+    pl.semaphore_wait(barrier, 19)
 
     def step_copy(o, source, target, which):
         return pltpu.make_async_remote_copy(
@@ -133,7 +174,7 @@
     rims = [
         pltpu.make_async_remote_copy(
             src_ref=ref.at[pl.ds(15, 1)],
-            dst_ref=joined.at[pl.ds(0, 1), :, pl.ds(low, size)],
+            dst_ref=rim.at[:, :, pl.ds(low, size)],
             send_sem=rim_send.at[k],
             recv_sem=rim_recv.at[k],
             device_id=(lax.rem(sp + 1, 16), dp),
@@ -143,29 +184,23 @@
     ]
     for copy in rims:
         copy.start()
-    out_load.start()
-    for copy in loads + gifts:
+    notes = [
+        pltpu.make_async_remote_copy(
+            src_ref=ref,
+            dst_ref=target.at[k + 1],
+            send_sem=name_send.at[which, k],
+            recv_sem=name_recv.at[which, k],
+            device_id=friend,
+            device_id_type=MESH,
+        )
+        for which, (ref, target) in enumerate(((ids, names), (shares, parts)))
+        for k, friend in enumerate((right, left, across))
+    ]
+    for copy in notes + gifts:
         copy.start()
-    for copy in own_loads:
-        copy.wait()
     for copy in rims:
         copy.wait_recv()
-
-    def convolve(cols, taps):
-        block = joined[:, :, cols].reshape(TOK + 8, 256).astype(F32)
-        block = jnp.where(iota((TOK + 8, 256), 0) + 8 * sp >= 8, block, 0.0)
-        running = taps[0:1] * block[5 : 5 + TOK]
-        for k in range(1, 4):
-            running = running + taps[k : k + 1] * block[5 + k : 5 + k + TOK]
-        conv[:, cols] = jax.nn.silu(running).astype(BF16)
-
-    def convolve_x(k):
-        cols = pl.ds(pl.multiple_of(k * 256, 256), 256)
-        convolve(cols, tap_x[:, cols])
-
-    each(0, 4, convolve_x)
-    convolve(pl.ds(INNER, 256), tap_b[...])
-    convolve(pl.ds(INNER + 256, 256), tap_c[...])
+    begin(convolve_rim)
 
     def wait_steps(o):
         step_copy(o, step_in, steps, 0).wait_recv()
@@ -256,7 +291,8 @@
                     total = term if total is None else total + term
                 inside[:, 64 * first : 64 * first + 128] = total
 
-    def placing_rows():
+    def placing_rows(j):
+        ids, shares = names[j], parts[j]
         expert = iota((16, TOK), 0)
         first, second = expert == ids[0:1, :], expert == ids[1:2, :]
         named = first | second
@@ -275,14 +311,18 @@
             ],
             axis=0,
         )
-        placing[...] = chosen.astype(BF16)
+        placing[j] = chosen.astype(BF16)
         rest = weights.T
         for k in range(3):
             piece = rest.astype(BF16)
-            weighing[pl.ds(TOK * k, TOK), :] = piece
+            weighing[j, pl.ds(TOK * k, TOK), :] = piece
             rest = rest - piece.astype(F32)
 
-    placing_rows()
+    placing_rows(0)
+    for copy in notes:
+        copy.wait_recv()
+    for j in range(1, 4):
+        placing_rows(j)
 
     def wait_state(o):
         decay_copy(o).wait_recv()
@@ -340,10 +380,10 @@
     out_load.wait()
 
     def project(k):
-        cols = pl.ds(pl.multiple_of(k * 256, 256), 256)
+        cols = pl.ds(pl.multiple_of(k * 512, 512), 512)
         pre[:, cols] = skip[:, cols].astype(F32) + dot(group_normed, out_v[:, cols])
 
-    each(0, width // 256, project)
+    each(0, width // 512, project)
 
     def standardize(k):
         rows = pl.ds(pl.multiple_of(k * 16, 16), 16)
@@ -352,14 +392,36 @@
         level = lax.rsqrt(jnp.mean(shifted * shifted, axis=1, keepdims=True) + norm_eps)
         normed[rows, :] = (shifted * level * gain[...] + offset[...]).astype(BF16)
 
-    each(0, TOK // 16, standardize)
+    far_cols = pl.ds(NEAR, width - NEAR)
+
+    def token_copy(lane, half):
+        rows = pl.ds(64 * half, 64)
+        if lane < 2:
+            source = normed.at[rows, far_cols]
+        else:
+            source = tokens.at[half, rows]
+        return pltpu.make_async_remote_copy(
+            src_ref=source,
+            dst_ref=tokens.at[lane, rows],
+            send_sem=token_send.at[lane, half],
+            recv_sem=token_recv.at[lane, half],
+            device_id=(right, left, (right, left)[half])[lane],
+            device_id_type=MESH,
+        )
+
+    each(0, TOK // 32, standardize)
+    token_copy(0, 0).start()
+    token_copy(1, 0).start()
+    each(TOK // 32, TOK // 16, standardize)
+    token_copy(1, 1).start()
+    token_copy(0, 1).start()
     flat_outgoing = outgoing.reshape(16 * SLOTS, width)
 
     def route(k):
-        cols = pl.ds(pl.multiple_of(k * 256, 256), 256)
-        flat_outgoing[:, cols] = dot(placing[...], normed[:, cols]).astype(BF16)
-
-    each(0, width // 256, route)
+        cols = pl.ds(pl.multiple_of(k * 512, 512), 512)
+        flat_outgoing[:, cols] = dot(placing[0], normed[:, cols]).astype(BF16)
+
+    each(0, width // 512, route)
 
     def go(o):
         return pltpu.make_async_remote_copy(
@@ -374,13 +436,15 @@
     each(1, 16, lambda o: go(o).start())
     gathered[0, 0:3] = outgoing[pl.ds(3 * sp, 3)]
 
+    near_cols = pl.ds(0, NEAR)
+
     def group(g):
         return pl.ds(12 * g, 12)
 
     def ring(src_slot, dst_slot, g, target, lane):
         return pltpu.make_async_remote_copy(
-            src_ref=gathered.at[src_slot, group(g)],
-            dst_ref=gathered.at[dst_slot, group(g)],
+            src_ref=gathered.at[src_slot, group(g), :, near_cols],
+            dst_ref=gathered.at[dst_slot, group(g), :, near_cols],
             send_sem=ring_send.at[lane, g],
             recv_sem=ring_recv.at[dst_slot - 1, g],
             device_id=target,
@@ -396,17 +460,59 @@
     def onward(g):
         return ring(1, 3, g, right, 2) if g < 2 else ring(2, 3, g, left, 2)
 
-    for g in range(4):
+    def far_copy(j, o):
+        return pltpu.make_async_remote_copy(
+            src_ref=far_rows.at[j - 1, pl.ds(3 * ahead(o), 3)],
+            dst_ref=gathered.at[j, pl.ds(3 * o, 3), :, far_cols],
+            send_sem=far_send.at[j - 1, o],
+            recv_sem=far_recv.at[j - 1, o],
+            device_id=(ahead(o), dp),
+            device_id_type=MESH,
+        )
+
+    def route_far(j):
+        flat = far_rows.at[j - 1].reshape(16 * SLOTS, width - NEAR)
+        flat[...] = dot(placing[j], tokens[j - 1]).astype(BF16)
+        each(1, 16, lambda o: far_copy(j, o).start())
+        gathered[j, 0:3, :, NEAR:] = far_rows[j - 1, pl.ds(3 * sp, 3)]
+
+    def wait_far(j, half):
+        each(max(8 * half, 1), 8 * half + 8, lambda o: far_copy(j, o).wait_recv())
+
+    def pass_on(g):
         each(max(4 * g, 1), 4 * g + 4, lambda o: go(o).wait_recv())
         to_right(g).start()
         to_left(g).start()
 
+    token_copy(0, 0).wait_recv()
+    token_copy(2, 0).start()
+    token_copy(1, 1).wait_recv()
+    token_copy(2, 1).start()
+    token_copy(0, 1).wait_recv()
+    route_far(1)
+    token_copy(1, 0).wait_recv()
+    route_far(2)
+    pass_on(0)
+    token_copy(2, 0).wait_recv()
+    token_copy(2, 1).wait_recv()
+    route_far(3)
+    pass_on(1)
     for copy in loads:
         copy.wait()
     for copy in gifts:
         copy.wait()
 
     tile = 256
+
+    def home_copy(j, o):
+        return pltpu.make_async_remote_copy(
+            src_ref=partial.at[j, pl.ds(3 * o, 3), :, far_cols],
+            dst_ref=far_answers.at[j, pl.ds(3 * sp, 3)],
+            send_sem=home_send.at[j, o],
+            recv_sem=home_recv.at[j, o],
+            device_id=(behind(o), dp),
+            device_id_type=MESH,
+        )
 
     def unit(slot, half):
         rows_here = gathered.at[slot, pl.ds(24 * half, 24)].reshape(192, width)
@@ -428,11 +534,14 @@
             ).astype(BF16)
 
         each(0, width // tile, down)
+        each(max(8 * half, 1), 8 * half + 8, lambda o: home_copy(slot, o).start())
+        if half == 0:
+            far_answers[slot, pl.ds(3 * sp, 3)] = partial[slot, 0:3, :, NEAR:]
 
     def sum_direct(slot, g):
         side = 0 if slot == 2 else 1
         return pltpu.make_async_remote_copy(
-            src_ref=partial.at[slot, group(g)],
+            src_ref=partial.at[slot, group(g), :, near_cols],
             dst_ref=summed.at[side, group(g)],
             send_sem=sum_send.at[side, g],
             recv_sem=sum_recv.at[side, g],
@@ -442,7 +551,7 @@
 
     def sum_relay(g):
         return pltpu.make_async_remote_copy(
-            src_ref=partial.at[3, group(g)],
+            src_ref=partial.at[3, group(g), :, near_cols],
             dst_ref=relayed.at[group(g)],
             send_sem=sum_send.at[2, g],
             recv_sem=sum_recv.at[2, g],
@@ -451,49 +560,100 @@
         )
 
     unit(0, 0)
+    pass_on(2)
+    pass_on(3)
     to_right(0).wait_recv()
     onward(0).start()
     unit(0, 1)
     to_right(1).wait_recv()
     onward(1).start()
+    wait_far(1, 0)
     unit(1, 0)
+    to_left(2).wait_recv()
+    onward(2).start()
     to_left(0).wait_recv()
     to_left(1).wait_recv()
+    wait_far(2, 0)
     unit(2, 0)
-    to_left(2).wait_recv()
-    onward(2).start()
     to_left(3).wait_recv()
     onward(3).start()
     sum_direct(1, 0).start()
     sum_direct(1, 1).start()
+    wait_far(2, 1)
     unit(2, 1)
     sum_direct(2, 2).start()
     sum_direct(2, 3).start()
     to_right(2).wait_recv()
     to_right(3).wait_recv()
+    wait_far(1, 1)
     unit(1, 1)
     onward(0).wait_recv()
     onward(1).wait_recv()
+    wait_far(3, 0)
     unit(3, 0)
     sum_relay(0).start()
     sum_relay(1).start()
     onward(2).wait_recv()
     onward(3).wait_recv()
+    wait_far(3, 1)
     unit(3, 1)
     sum_relay(2).start()
     sum_relay(3).start()
-    for g in (0, 2, 1, 3):
+
+    def combine(j):
+        each(1, 16, lambda o: home_copy(j, o).wait_recv())
+        flat = far_answers.at[j].reshape(16 * SLOTS, width - NEAR)
+        terms = dot(weighing[j], flat[...])
+        return terms[0:TOK] + terms[TOK : 2 * TOK] + terms[2 * TOK : 3 * TOK]
+
+    def tsum_copy(lane, half):
+        rows = pl.ds(64 * half, 64)
+        if lane == 2:
+            source, target = token_out.at[2, rows], token_relay.at[rows]
+            device = (right, left)[half]
+        else:
+            source, target = token_out.at[lane, rows], token_in.at[lane, rows]
+            device = (right, left)[lane]
+        return pltpu.make_async_remote_copy(
+            src_ref=source,
+            dst_ref=target,
+            send_sem=tsum_send.at[lane, half],
+            recv_sem=tsum_recv.at[lane, half],
+            device_id=device,
+            device_id_type=MESH,
+        )
+
+    def relay_add(g):
         slot = 2 if g < 2 else 1
         sum_relay(g).wait_recv()
-        partial[slot, group(g)] = (
-            partial[slot, group(g)].astype(F32)
-            + relayed[group(g)].astype(F32)
+        partial[slot, group(g), :, 0:NEAR] = (
+            partial[slot, group(g), :, 0:NEAR].astype(F32) + relayed[group(g)].astype(F32)
         ).astype(BF16)
         sum_direct(slot, g).start()
 
+    token_out[1] = combine(1).astype(BF16)
+    tsum_copy(1, 0).start()
+    token_out[0] = combine(2).astype(BF16)
+    tsum_copy(0, 1).start()
+    relay_add(0)
+    relay_add(2)
+    token_out[2] = combine(3).astype(BF16)
+    tsum_copy(2, 0).start()
+    tsum_copy(2, 1).start()
+    token_sum[...] = combine(0)
+    relay_add(1)
+    relay_add(3)
+    for half in range(2):
+        lane, rows = half, pl.ds(64 * half, 64)
+        tsum_copy(2, half).wait_recv()
+        token_out[lane, rows] = (
+            token_out[lane, rows].astype(F32) + token_relay[rows].astype(F32)
+        ).astype(BF16)
+        tsum_copy(lane, half).start()
+
     def back(o):
         return pltpu.make_async_remote_copy(
-            src_ref=partial.at[0, pl.ds(3 * o, 3)],
+            src_ref=partial.at[0, pl.ds(3 * o, 3), :, near_cols],
             dst_ref=answers.at[pl.ds(3 * sp, 3)],
             send_sem=back_send.at[o],
             recv_sem=back_recv.at[o],
@@ -504,17 +664,29 @@
     for g in (0, 2, 1, 3):
         sum_direct(2, g).wait_recv()
         sum_direct(1, g).wait_recv()
-        partial[0, group(g)] = (
-            partial[0, group(g)].astype(F32)
+        partial[0, group(g), :, 0:NEAR] = (
+            partial[0, group(g), :, 0:NEAR].astype(F32)
             + summed[0, group(g)].astype(F32)
             + summed[1, group(g)].astype(F32)
         ).astype(BF16)
         each(max(4 * g, 1), 4 * g + 4, lambda o: back(o).start())
         if g == 0:
-            answers[pl.ds(3 * sp, 3)] = partial[0, 0:3]
-
-    for copy in rims:
+            answers[pl.ds(3 * sp, 3)] = partial[0, 0:3, :, 0:NEAR]
+
+    for copy in rims + notes:
         copy.wait_send()
+    for lane in range(3):
+        for half in range(2):
+            token_copy(lane, half).wait_send()
+            tsum_copy(lane, half).wait_send()
+            if lane < 2:
+                tsum_copy(lane, half).wait_recv()
+    result[:, NEAR:] = (
+        normed[:, NEAR:].astype(F32)
+        + token_sum[...]
+        + token_in[0].astype(F32)
+        + token_in[1].astype(F32)
+    ).astype(BF16)
     for g in range(4):
         to_right(g).wait_send()
         to_left(g).wait_send()
@@ -530,19 +702,23 @@
         state_copy(o).wait_send()
         enter_copy(o).wait_send()
         go(o).wait_send()
+        for j in range(4):
+            if j > 0:
+                far_copy(j, o).wait_send()
+            home_copy(j, o).wait_send()
         back(o).wait_send()
         back(o).wait_recv()
 
     each(1, 16, drain)
-    flat_answers = answers.reshape(16 * SLOTS, width)
+    flat_answers = answers.reshape(16 * SLOTS, NEAR)
 
     def finish(k):
         cols = pl.ds(pl.multiple_of(k * 256, 256), 256)
-        terms = dot(weighing[...], flat_answers[:, cols])
+        terms = dot(weighing[0], flat_answers[:, cols])
         routed = terms[0:TOK] + terms[TOK : 2 * TOK] + terms[2 * TOK : 3 * TOK]
         result[:, cols] = (normed[:, cols].astype(F32) + routed).astype(BF16)
 
-    each(0, width // 256, finish)
+    each(0, NEAR // 256, finish)
 
 
 def per_device(
@@ -574,15 +750,19 @@
     scalars = pl.BlockSpec(memory_space=pltpu.SMEM)
     dma = pltpu.SemaphoreType.DMA
     rows = 2 * SLOTS
+    rest = width - NEAR
     out = pl.pallas_call(
         layer_kernel,
         out_shape=jax.ShapeDtypeStruct((TOK, width), BF16),
-        in_specs=[scalars, near, near] + [far] * 5 + [near] * 4 + [far] + [near] * 4 + [far] * 3,
+        in_specs=[scalars, near, near] + [far] * 5 + [near] * 4 + [far] + [near] * 2 + [far] * 5,
         out_specs=near,
         scratch_shapes=[
-            pltpu.VMEM((17, 8, 1536), BF16),
+            pltpu.VMEM((16, 8, 1536), BF16),
+            pltpu.VMEM((1, 8, 1536), BF16),
             pltpu.VMEM((HEADS, 1, TOK), F32),
             pltpu.VMEM((HEADS, 1, TOK), F32),
+            pltpu.VMEM((4, 2, TOK), jnp.int32),
+            pltpu.VMEM((4, 2, TOK), F32),
             pltpu.VMEM((TOK, 1536), BF16),
             pltpu.VMEM((64, INNER), F32),
             pltpu.VMEM((2, 1, 512), F32),
@@ -594,21 +774,30 @@
             pltpu.VMEM((INNER, width), BF16),
             pltpu.VMEM((TOK, width), F32),
             pltpu.VMEM((TOK, width), BF16),
-            pltpu.VMEM((16 * SLOTS, TOK), BF16),
-            pltpu.VMEM((3 * TOK, 16 * SLOTS), BF16),
+            pltpu.VMEM((4, 16 * SLOTS, TOK), BF16),
+            pltpu.VMEM((4, 3 * TOK, 16 * SLOTS), BF16),
             pltpu.VMEM((rows, 8, width), BF16),
-            pltpu.VMEM((rows, 8, width), BF16),
+            pltpu.VMEM((rows, 8, NEAR), BF16),
+            pltpu.VMEM((3, TOK, rest), BF16),
+            pltpu.VMEM((3, rows, 8, rest), BF16),
+            pltpu.VMEM((4, rows, 8, rest), BF16),
+            pltpu.VMEM((TOK, rest), F32),
+            pltpu.VMEM((3, TOK, rest), BF16),
+            pltpu.VMEM((TOK, rest), BF16),
+            pltpu.VMEM((2, TOK, rest), BF16),
             pltpu.VMEM((4, rows, 8, width), BF16),
             pltpu.VMEM((4, rows, 8, width), BF16),
-            pltpu.VMEM((rows, 8, width), BF16),
-            pltpu.VMEM((2, rows, 8, width), BF16),
+            pltpu.VMEM((rows, 8, NEAR), BF16),
+            pltpu.VMEM((2, rows, 8, NEAR), BF16),
             pltpu.VMEM((width, 2 * part), BF16),
             pltpu.VMEM((width, 2 * part), BF16),
             pltpu.VMEM((2 * part, width), BF16),
             pltpu.VMEM((192, 2 * part), BF16),
-            dma((6,)), dma((3,)), dma((3,)), dma((2, 16)), dma((2, 16)), dma((2, 16)), dma((2, 16)),
+            dma((8,)), dma((3,)), dma((3,)), dma((2, 3)), dma((2, 3)), dma((2, 16)), dma((2, 16)), dma((2, 16)), dma((2, 16)),
             dma((16,)), dma((16,)), dma((3,)), dma((3,)), dma((3,)), dma((16,)), dma((16,)),
             dma((3, 4)), dma((3, 4)), dma((3, 4)), dma((3, 4)), dma((16,)), dma((16,)),
+            dma((3, 2)), dma((3, 2)), dma((3, 16)), dma((3, 16)), dma((4, 16)), dma((4, 16)),
+            dma((3, 2)), dma((3, 2)),
         ],
         compiler_params=pltpu.CompilerParams(
             collective_id=0, has_side_effects=True, vmem_limit_bytes=62 * 1024 * 1024

time: 157 us -> 133 us (0.85)
  Pallas kernels: 155 us -> 130 us
    pallas_call x1, Pallas kernels: 155 us -> 130 us  [per_device(): pl.pallas_call(layer_kernel, out_shape=jax.ShapeDtypeStruct((TOK, width),...]
where the time goes in v2:
time: 133 us; the launch traced here: 132 us
  Pallas kernels  130 us (98%)
  local copies, waits for them, and re-layouts  1.88 us (1%)
    pallas_call x1, Pallas kernels, per_device(): pl.pallas_call(layer_kernel, out_shape=jax.ShapeDtypeStruct((TOK, width),...  130 us

profile of v2, /device:TPU:0, one launch (start us, length us, event | category | flops | bytes accessed | tf_op | source)
XLA Modules:
  0.0 132.1 jit_solution(1645009742502042174)
XLA Ops:
  0.0 130.2 %layer.1 = bf16[128,2048]{1,0:T(8,128)(2,1)} custom-call(f32[16]{0:T(128)} %speed.1, bf16[128,2048]{1,0:T(8,128)(2,1)} %bitcast.24, bf16[128,1024]{1,0:T(8,128)(2,1)} %bitcast.25, bf16[16,8,1024]{2,1,0:T(8,128)(2,1)} %bitcast.26, bf16[16,8,256]{2,1,0:T(8,128)(2,1)} %bitcast.27, bf16[16,8,256]{2,1,0:T(8,128)(2,1)} %bitcast.28, f32[16,1,128]{2,1,0:T(1,128)} %bitcast.29, ...), custom_call_target="tpu_custom_call" | custom-call | tf_op jit(solution)/shard_map/layer/pallas_call | solution.py:754
  130.2 1.9 %copy.22 = bf16[1,128,2048]{2,1,0:T(8,128)(2,1)} copy(bf16[1,128,2048]{2,1,0:T(8,128)(2,1)} %bitcast.23) | data formatting | bytes 1048576

commit v3 on v2

--- a/solution.py
+++ b/solution.py
@@ -34,10 +34,10 @@
 
 
 def layer_kernel(
-    speed, skip, valve, chan, hid, probe, step_in, fade_in, tap_x, tap_b, tap_c, group_gain, out_w,
+    speed, skip_in, valve_in, chan, hid, probe, step_in, fade_in, tap_x, tap_b, tap_c, group_gain, out_w,
     gain, offset, ids, shares, gate_w, raise_w, lower_w,
     result,
-    joined, rim, steps, fades, names, parts, conv, state, decay, state_in, decay_in, entering,
+    skip, valve, joined, rim, steps_out, fades_out, steps, fades, names, parts, conv, state, decay, state_in, decay_in, entering,
     entered, inside, out_v, pre, normed, placing, weighing, outgoing, answers,
     tokens, far_rows, far_answers, token_sum, token_out, token_relay, token_in,
     gathered, partial, relayed, summed, gate_v, raise_v, lower_v, hidden,
@@ -55,7 +55,7 @@
     left = (sp, lax.rem(x + 3, 4) * 2 + core)
     across = (sp, lax.rem(x + 2, 4) * 2 + core)
     twin = (sp, x * 2 + 1 - core)
-    width = skip.shape[1]
+    width = skip_in.shape[1]
     part = gate_w.shape[1]
 
     def ahead(o):
@@ -90,15 +90,15 @@
         )
         for k, (ref, low, size) in enumerate(spans)
     ]
-    own_loads.append(
-        pltpu.make_async_copy(step_in.at[sp], steps.at[sp], load_sem.at[3])
-    )
-    own_loads.append(
-        pltpu.make_async_copy(fade_in.at[sp], fades.at[sp], load_sem.at[4])
-    )
+    own_loads.append(pltpu.make_async_copy(step_in, steps_out, load_sem.at[3]))
+    own_loads.append(pltpu.make_async_copy(fade_in, fades_out, load_sem.at[4]))
     own_loads.append(pltpu.make_async_copy(ids, names.at[0], load_sem.at[6]))
     own_loads.append(pltpu.make_async_copy(shares, parts.at[0], load_sem.at[7]))
     out_load = pltpu.make_async_copy(out_w, out_v, load_sem.at[5])
+    late_loads = [
+        pltpu.make_async_copy(skip_in, skip, load_sem.at[8]),
+        pltpu.make_async_copy(valve_in, valve, load_sem.at[9]),
+    ]
     for copy in own_loads:
         copy.start()
     loads, gifts = [], []
@@ -121,11 +121,13 @@
             )
         )
 
+    for copy in own_loads:
+        copy.wait()
+    for copy in late_loads:
+        copy.start()
     out_load.start()
     for copy in loads:
         copy.start()
-    for copy in own_loads:
-        copy.wait()
 
     def filtered(block, taps):
         high = block.shape[0] - 8
@@ -167,33 +169,35 @@
         )
 
     def send_steps(o):
-        step_copy(o, step_in, steps, 0).start()
-        step_copy(o, fade_in, fades, 1).start()
+        step_copy(o, steps_out, steps, 0).start()
+        step_copy(o, fades_out, fades, 1).start()
 
     each(1, 16, send_steps)
+    steps[sp] = steps_out[sp]
+    fades[sp] = fades_out[sp]
     rims = [
         pltpu.make_async_remote_copy(
-            src_ref=ref.at[pl.ds(15, 1)],
+            src_ref=joined.at[pl.ds(15, 1), :, pl.ds(low, size)],
             dst_ref=rim.at[:, :, pl.ds(low, size)],
             send_sem=rim_send.at[k],
             recv_sem=rim_recv.at[k],
             device_id=(lax.rem(sp + 1, 16), dp),
             device_id_type=MESH,
         )
-        for k, (ref, low, size) in enumerate(spans)
+        for k, (_, low, size) in enumerate(spans)
     ]
     for copy in rims:
         copy.start()
     notes = [
         pltpu.make_async_remote_copy(
-            src_ref=ref,
+            src_ref=target.at[0],
             dst_ref=target.at[k + 1],
             send_sem=name_send.at[which, k],
             recv_sem=name_recv.at[which, k],
             device_id=friend,
             device_id_type=MESH,
         )
-        for which, (ref, target) in enumerate(((ids, names), (shares, parts)))
+        for which, target in enumerate((names, parts))
         for k, friend in enumerate((right, left, across))
     ]
     for copy in notes + gifts:
@@ -203,8 +207,8 @@
     begin(convolve_rim)
 
     def wait_steps(o):
-        step_copy(o, step_in, steps, 0).wait_recv()
-        step_copy(o, fade_in, fades, 1).wait_recv()
+        step_copy(o, steps_out, steps, 0).wait_recv()
+        step_copy(o, fades_out, fades, 1).wait_recv()
 
     each(1, 16, wait_steps)
     row = iota((HEADS, TOK), 0)
@@ -225,19 +229,19 @@
     last = cum_col[TOK - 1 : TOK]
     tail_wide = dot(jnp.exp(last - cum_col) * step_col, spread, EXACT)
     decay_wide = dot(jnp.broadcast_to(jnp.exp(last), (8, HEADS)), spread, EXACT)
-    for k in range(2):
-        decay[k] = decay_wide[0:1, 512 * k : 512 * k + 512]
+    for k in range(4):
+        decay[k] = decay_wide[0:1, 256 * k : 256 * k + 256]
     scaled = (conv[:, 0:INNER].astype(F32) * tail_wide).astype(BF16)
     for q in range(2):
         b_pair = conv[:, INNER + 128 * q : INNER + 128 * q + 128]
         both = dot(b_pair.T, scaled[:, 512 * q : 512 * q + 512])
-        state[:, 512 * q : 512 * q + 256] = both[0:64, 0:256]
-        state[:, 512 * q + 256 : 512 * q + 512] = both[64:128, 256:512]
+        state[:, 512 * q : 512 * q + 256] = both[0:64, 0:256].astype(BF16)
+        state[:, 512 * q + 256 : 512 * q + 512] = both[64:128, 256:512].astype(BF16)
 
     def place_of(k):
         return (
-            pl.ds(pl.multiple_of(lax.div(k, 2) * 8, 8), 8),
-            pl.ds(pl.multiple_of(lax.rem(k, 2) * 512, 512), 512),
+            pl.ds(pl.multiple_of(lax.div(k, 4) * 16, 16), 16),
+            pl.ds(pl.multiple_of(lax.rem(k, 4) * 256, 256), 256),
         )
 
     def state_copy(o):
@@ -253,7 +257,7 @@
 
     def decay_copy(o):
         return pltpu.make_async_remote_copy(
-            src_ref=decay.at[lax.rem(ahead(o), 2)],
+            src_ref=decay.at[lax.rem(ahead(o), 4)],
             dst_ref=decay_in.at[sp],
             send_sem=state_send.at[1, o],
             recv_sem=state_recv.at[1, o],
@@ -268,7 +272,7 @@
     each(1, 16, send_state)
     my_rows, my_cols = place_of(sp)
     state_in[sp] = state[my_rows, my_cols]
-    decay_in[sp] = decay[lax.rem(sp, 2)]
+    decay_in[sp] = decay[lax.rem(sp, 4)]
 
     low_half = iota((TOK, TOK), 1) < 64
     for q in range(2):
@@ -313,7 +317,7 @@
         )
         placing[j] = chosen.astype(BF16)
         rest = weights.T
-        for k in range(3):
+        for k in range(2):
             piece = rest.astype(BF16)
             weighing[j, pl.ds(TOK * k, TOK), :] = piece
             rest = rest - piece.astype(F32)
@@ -331,10 +335,10 @@
     each(1, 16, wait_state)
 
     def advance(j, held):
-        entering[j] = held
-        return decay_in[j] * held + state_in[j]
-
-    lax.fori_loop(0, 16, advance, jnp.zeros((8, 512), F32))
+        entering[j] = held.astype(BF16)
+        return decay_in[j] * held + state_in[j].astype(F32)
+
+    lax.fori_loop(0, 16, advance, jnp.zeros((16, 256), F32))
 
     def enter_copy(o):
         rows, cols = place_of(sp)
@@ -352,7 +356,9 @@
     reach_wide = dot(jnp.exp(cum_col), spread, EXACT)
     each(1, 16, lambda o: enter_copy(o).wait_recv())
 
-    nothing = jnp.zeros((64, 256), F32)
+    for copy in late_loads:
+        copy.wait()
+    nothing = jnp.zeros((64, 256), BF16)
     blocks = []
     for q in range(2):
         c_pair = conv[:, INNER + 256 + 128 * q : INNER + 256 + 128 * q + 128]
@@ -364,7 +370,7 @@
             ],
             axis=0,
         )
-        carried = dot(c_pair.astype(F32), both, EXACT)
+        carried = dot(c_pair, both)
         for g in range(2):
             low_col = 512 * q + 256 * g
             mixed = (
@@ -386,7 +392,7 @@
     each(0, width // 512, project)
 
     def standardize(k):
-        rows = pl.ds(pl.multiple_of(k * 16, 16), 16)
+        rows = pl.ds(64 * k, 64)
         block = pre[rows, :]
         shifted = block - jnp.mean(block, axis=1, keepdims=True)
         level = lax.rsqrt(jnp.mean(shifted * shifted, axis=1, keepdims=True) + norm_eps)
@@ -409,10 +415,10 @@
             device_id_type=MESH,
         )
 
-    each(0, TOK // 32, standardize)
+    standardize(0)
     token_copy(0, 0).start()
     token_copy(1, 0).start()
-    each(TOK // 32, TOK // 16, standardize)
+    standardize(1)
     token_copy(1, 1).start()
     token_copy(0, 1).start()
     flat_outgoing = outgoing.reshape(16 * SLOTS, width)
@@ -515,27 +521,20 @@
         )
 
     def unit(slot, half):
-        rows_here = gathered.at[slot, pl.ds(24 * half, 24)].reshape(192, width)
-        block = rows_here[...]
-
-        def up(k):
-            cols = pl.ds(pl.multiple_of(k * tile, tile), tile)
-            gate_val = jnp.dot(block, gate_v[:, cols], preferred_element_type=F32)
-            up_val = jnp.dot(block, raise_v[:, cols], preferred_element_type=F32)
+        block = gathered.at[slot, pl.ds(24 * half, 24)].reshape(192, width)
+        for k in range(2 * part // tile):
+            cols = pl.ds(k * tile, tile)
+            gate_val = dot(block[...], gate_v[:, cols])
+            up_val = dot(block[...], raise_v[:, cols])
             hidden[:, cols] = (jax.nn.silu(gate_val) * up_val).astype(BF16)
-
-        each(0, 2 * part // tile, up)
         target = partial.at[slot, pl.ds(24 * half, 24)].reshape(192, width)
-
-        def down(k):
-            cols = pl.ds(pl.multiple_of(k * tile, tile), tile)
-            target[:, cols] = jnp.dot(
-                hidden[...], lower_v[:, cols], preferred_element_type=F32
-            ).astype(BF16)
-
-        each(0, width // tile, down)
-        each(max(8 * half, 1), 8 * half + 8, lambda o: home_copy(slot, o).start())
-        if half == 0:
+        for k in range(width // tile):
+            cols = pl.ds(k * tile, tile)
+            target[:, cols] = dot(hidden[...], lower_v[:, cols]).astype(BF16)
+        each(jnp.maximum(8 * half, 1), 8 * half + 8, lambda o: home_copy(slot, o).start())
+
+        @pl.when(half == 0)
+        def _():
             far_answers[slot, pl.ds(3 * sp, 3)] = partial[slot, 0:3, :, NEAR:]
 
     def sum_direct(slot, g):
@@ -559,52 +558,11 @@
             device_id_type=MESH,
         )
 
-    unit(0, 0)
-    pass_on(2)
-    pass_on(3)
-    to_right(0).wait_recv()
-    onward(0).start()
-    unit(0, 1)
-    to_right(1).wait_recv()
-    onward(1).start()
-    wait_far(1, 0)
-    unit(1, 0)
-    to_left(2).wait_recv()
-    onward(2).start()
-    to_left(0).wait_recv()
-    to_left(1).wait_recv()
-    wait_far(2, 0)
-    unit(2, 0)
-    to_left(3).wait_recv()
-    onward(3).start()
-    sum_direct(1, 0).start()
-    sum_direct(1, 1).start()
-    wait_far(2, 1)
-    unit(2, 1)
-    sum_direct(2, 2).start()
-    sum_direct(2, 3).start()
-    to_right(2).wait_recv()
-    to_right(3).wait_recv()
-    wait_far(1, 1)
-    unit(1, 1)
-    onward(0).wait_recv()
-    onward(1).wait_recv()
-    wait_far(3, 0)
-    unit(3, 0)
-    sum_relay(0).start()
-    sum_relay(1).start()
-    onward(2).wait_recv()
-    onward(3).wait_recv()
-    wait_far(3, 1)
-    unit(3, 1)
-    sum_relay(2).start()
-    sum_relay(3).start()
-
     def combine(j):
         each(1, 16, lambda o: home_copy(j, o).wait_recv())
         flat = far_answers.at[j].reshape(16 * SLOTS, width - NEAR)
         terms = dot(weighing[j], flat[...])
-        return terms[0:TOK] + terms[TOK : 2 * TOK] + terms[2 * TOK : 3 * TOK]
+        return terms[0:TOK] + terms[TOK : 2 * TOK]
 
     def tsum_copy(lane, half):
         rows = pl.ds(64 * half, 64)
@@ -631,26 +589,77 @@
         ).astype(BF16)
         sum_direct(slot, g).start()
 
+    def before_own():
+        pass_on(2)
+        pass_on(3)
+        to_right(0).wait_recv()
+        onward(0).start()
+
+    def before_left():
+        to_right(1).wait_recv()
+        onward(1).start()
+        wait_far(1, 0)
+
+    def before_right():
+        to_left(0).wait_recv()
+        to_left(1).wait_recv()
+        wait_far(2, 0)
+
+    def before_right_rest():
+        to_left(2).wait_recv()
+        onward(2).start()
+        to_left(3).wait_recv()
+        onward(3).start()
+        sum_direct(1, 0).start()
+        sum_direct(1, 1).start()
+        wait_far(2, 1)
+
+    def before_left_rest():
+        sum_direct(2, 2).start()
+        sum_direct(2, 3).start()
+        to_right(2).wait_recv()
+        to_right(3).wait_recv()
+        wait_far(1, 1)
+
+    def before_across():
+        token_sum[...] = combine(0)
+        onward(0).wait_recv()
+        onward(1).wait_recv()
+        wait_far(3, 0)
+
+    def before_across_rest():
+        sum_relay(0).start()
+        sum_relay(1).start()
+        token_out[0] = combine(2).astype(BF16)
+        onward(2).wait_recv()
+        onward(3).wait_recv()
+        wait_far(3, 1)
+
+    befores = (
+        before_own, before_left, before_right, before_right_rest, before_left_rest,
+        before_across, before_across_rest,
+    )
+
+    def turn(u):
+        for k, before in enumerate(befores):
+            pl.when(u == k + 1)(before)
+        slot = jnp.where(u < 2, 0, jnp.where(u >= 6, 3, jnp.where((u == 2) | (u == 5), 1, 2)))
+        half = jnp.where((u == 1) | (u == 4) | (u == 5) | (u == 7), 1, 0)
+        unit(slot, half)
+
+    each(0, 8, turn)
+    sum_relay(2).start()
+    sum_relay(3).start()
     token_out[1] = combine(1).astype(BF16)
-    tsum_copy(1, 0).start()
-    token_out[0] = combine(2).astype(BF16)
-    tsum_copy(0, 1).start()
     relay_add(0)
     relay_add(2)
+    tsum_copy(0, 1).start()
+    tsum_copy(1, 0).start()
     token_out[2] = combine(3).astype(BF16)
+    relay_add(1)
+    relay_add(3)
     tsum_copy(2, 0).start()
     tsum_copy(2, 1).start()
-    token_sum[...] = combine(0)
-    relay_add(1)
-    relay_add(3)
-    for half in range(2):
-        lane, rows = half, pl.ds(64 * half, 64)
-        tsum_copy(2, half).wait_recv()
-        token_out[lane, rows] = (
-            token_out[lane, rows].astype(F32) + token_relay[rows].astype(F32)
-        ).astype(BF16)
-        tsum_copy(lane, half).start()
-
     def back(o):
         return pltpu.make_async_remote_copy(
             src_ref=partial.at[0, pl.ds(3 * o, 3), :, near_cols],
@@ -672,6 +681,14 @@
         each(max(4 * g, 1), 4 * g + 4, lambda o: back(o).start())
         if g == 0:
             answers[pl.ds(3 * sp, 3)] = partial[0, 0:3, :, 0:NEAR]
+
+    for half in range(2):
+        lane, rows = half, pl.ds(64 * half, 64)
+        tsum_copy(2, half).wait_recv()
+        token_out[lane, rows] = (
+            token_out[lane, rows].astype(F32) + token_relay[rows].astype(F32)
+        ).astype(BF16)
+        tsum_copy(lane, half).start()
 
     for copy in rims + notes:
         copy.wait_send()
@@ -696,8 +713,8 @@
         sum_relay(g).wait_send()
 
     def drain(o):
-        step_copy(o, step_in, steps, 0).wait_send()
-        step_copy(o, fade_in, fades, 1).wait_send()
+        step_copy(o, steps_out, steps, 0).wait_send()
+        step_copy(o, fades_out, fades, 1).wait_send()
         decay_copy(o).wait_send()
         state_copy(o).wait_send()
         enter_copy(o).wait_send()
@@ -715,7 +732,7 @@
     def finish(k):
         cols = pl.ds(pl.multiple_of(k * 256, 256), 256)
         terms = dot(weighing[0], flat_answers[:, cols])
-        routed = terms[0:TOK] + terms[TOK : 2 * TOK] + terms[2 * TOK : 3 * TOK]
+        routed = terms[0:TOK] + terms[TOK : 2 * TOK]
         result[:, cols] = (normed[:, cols].astype(F32) + routed).astype(BF16)
 
     each(0, NEAR // 256, finish)
@@ -754,28 +771,32 @@
     out = pl.pallas_call(
         layer_kernel,
         out_shape=jax.ShapeDtypeStruct((TOK, width), BF16),
-        in_specs=[scalars, near, near] + [far] * 5 + [near] * 4 + [far] + [near] * 2 + [far] * 5,
+        in_specs=[scalars] + [far] * 7 + [near] * 4 + [far] + [near] * 2 + [far] * 5,
         out_specs=near,
         scratch_shapes=[
+            pltpu.VMEM((TOK, width), BF16),
+            pltpu.VMEM((TOK, INNER), BF16),
             pltpu.VMEM((16, 8, 1536), BF16),
             pltpu.VMEM((1, 8, 1536), BF16),
+            pltpu.VMEM((HEADS, 1, TOK), F32),
+            pltpu.VMEM((HEADS, 1, TOK), F32),
             pltpu.VMEM((HEADS, 1, TOK), F32),
             pltpu.VMEM((HEADS, 1, TOK), F32),
             pltpu.VMEM((4, 2, TOK), jnp.int32),
             pltpu.VMEM((4, 2, TOK), F32),
             pltpu.VMEM((TOK, 1536), BF16),
-            pltpu.VMEM((64, INNER), F32),
-            pltpu.VMEM((2, 1, 512), F32),
-            pltpu.VMEM((16, 8, 512), F32),
-            pltpu.VMEM((16, 1, 512), F32),
-            pltpu.VMEM((16, 8, 512), F32),
-            pltpu.VMEM((64, INNER), F32),
+            pltpu.VMEM((64, INNER), BF16),
+            pltpu.VMEM((4, 1, 256), F32),
+            pltpu.VMEM((16, 16, 256), BF16),
+            pltpu.VMEM((16, 1, 256), F32),
+            pltpu.VMEM((16, 16, 256), BF16),
+            pltpu.VMEM((64, INNER), BF16),
             pltpu.VMEM((TOK, INNER), F32),
             pltpu.VMEM((INNER, width), BF16),
             pltpu.VMEM((TOK, width), F32),
             pltpu.VMEM((TOK, width), BF16),
             pltpu.VMEM((4, 16 * SLOTS, TOK), BF16),
-            pltpu.VMEM((4, 3 * TOK, 16 * SLOTS), BF16),
+            pltpu.VMEM((4, 2 * TOK, 16 * SLOTS), BF16),
             pltpu.VMEM((rows, 8, width), BF16),
             pltpu.VMEM((rows, 8, NEAR), BF16),
             pltpu.VMEM((3, TOK, rest), BF16),
@@ -793,7 +814,7 @@
             pltpu.VMEM((width, 2 * part), BF16),
             pltpu.VMEM((2 * part, width), BF16),
             pltpu.VMEM((192, 2 * part), BF16),
-            dma((8,)), dma((3,)), dma((3,)), dma((2, 3)), dma((2, 3)), dma((2, 16)), dma((2, 16)), dma((2, 16)), dma((2, 16)),
+            dma((10,)), dma((3,)), dma((3,)), dma((2, 3)), dma((2, 3)), dma((2, 16)), dma((2, 16)), dma((2, 16)), dma((2, 16)),
             dma((16,)), dma((16,)), dma((3,)), dma((3,)), dma((3,)), dma((16,)), dma((16,)),
             dma((3, 4)), dma((3, 4)), dma((3, 4)), dma((3, 4)), dma((16,)), dma((16,)),
             dma((3, 2)), dma((3, 2)), dma((3, 16)), dma((3, 16)), dma((4, 16)), dma((4, 16)),

time: 133 us -> 124 us (0.932)
  Pallas kernels: 130 us -> 121 us
    pallas_call x1, Pallas kernels: 130 us -> 121 us  [per_device(): pl.pallas_call(layer_kernel, out_shape=jax.ShapeDtypeStruct((TOK, width),...]
where the time goes in v3:
time: 124 us; the launch traced here: 123 us
  Pallas kernels  121 us (98%)
  local copies, waits for them, and re-layouts  1.88 us (2%)
    pallas_call x1, Pallas kernels, per_device(): pl.pallas_call(layer_kernel, out_shape=jax.ShapeDtypeStruct((TOK, width),...  121 us

profile of v3, /device:TPU:0, one launch (start us, length us, event | category | flops | bytes accessed | tf_op | source)
XLA Modules:
  0.0 123.3 jit_solution(4372105820985268126)
XLA Ops:
  0.0 121.4 %layer.1 = bf16[128,2048]{1,0:T(8,128)(2,1)} custom-call(f32[16]{0:T(128)} %speed.1, bf16[128,2048]{1,0:T(8,128)(2,1)} %bitcast.24, bf16[128,1024]{1,0:T(8,128)(2,1)} %bitcast.25, bf16[16,8,1024]{2,1,0:T(8,128)(2,1)} %bitcast.26, bf16[16,8,256]{2,1,0:T(8,128)(2,1)} %bitcast.27, bf16[16,8,256]{2,1,0:T(8,128)(2,1)} %bitcast.28, f32[16,1,128]{2,1,0:T(1,128)} %bitcast.29, ...), custom_call_target="tpu_custom_call" | custom-call | tf_op jit(solution)/shard_map/layer/pallas_call | solution.py:771
  121.4 1.9 %copy.22 = bf16[1,128,2048]{2,1,0:T(8,128)(2,1)} copy(bf16[1,128,2048]{2,1,0:T(8,128)(2,1)} %bitcast.23) | data formatting | bytes 1048576

commit v4 on v3

--- a/solution.py
+++ b/solution.py
@@ -11,7 +11,8 @@
 TOK = 128
 INNER = 1024
 SLOTS = 24
-NEAR = 1280
+NEAR = 1152
+NEAR_BACK = 1152
 rms_eps = 1e-06
 norm_eps = 1e-05
 BF16 = jnp.bfloat16
@@ -386,10 +387,11 @@
     out_load.wait()
 
     def project(k):
-        cols = pl.ds(pl.multiple_of(k * 512, 512), 512)
+        cols = pl.ds(512 * k, 512)
         pre[:, cols] = skip[:, cols].astype(F32) + dot(group_normed, out_v[:, cols])
 
-    each(0, width // 512, project)
+    for k in range(width // 512):
+        project(k)
 
     def standardize(k):
         rows = pl.ds(64 * k, 64)
@@ -424,10 +426,11 @@
     flat_outgoing = outgoing.reshape(16 * SLOTS, width)
 
     def route(k):
-        cols = pl.ds(pl.multiple_of(k * 512, 512), 512)
+        cols = pl.ds(512 * k, 512)
         flat_outgoing[:, cols] = dot(placing[0], normed[:, cols]).astype(BF16)
 
-    each(0, width // 512, route)
+    for k in range(width // 512):
+        route(k)
 
     def go(o):
         return pltpu.make_async_remote_copy(
@@ -443,6 +446,8 @@
     gathered[0, 0:3] = outgoing[pl.ds(3 * sp, 3)]
 
     near_cols = pl.ds(0, NEAR)
+    near_back = pl.ds(0, NEAR_BACK)
+    far_back = pl.ds(NEAR_BACK, width - NEAR_BACK)
 
     def group(g):
         return pl.ds(12 * g, 12)
@@ -479,8 +484,10 @@
     def route_far(j):
         flat = far_rows.at[j - 1].reshape(16 * SLOTS, width - NEAR)
         flat[...] = dot(placing[j], tokens[j - 1]).astype(BF16)
-        each(1, 16, lambda o: far_copy(j, o).start())
         gathered[j, 0:3, :, NEAR:] = far_rows[j - 1, pl.ds(3 * sp, 3)]
+
+    def send_far(j, half):
+        each(max(8 * half, 1), 8 * half + 8, lambda o: far_copy(j, o).start())
 
     def wait_far(j, half):
         each(max(8 * half, 1), 8 * half + 8, lambda o: far_copy(j, o).wait_recv())
@@ -496,12 +503,18 @@
     token_copy(2, 1).start()
     token_copy(0, 1).wait_recv()
     route_far(1)
+    send_far(1, 0)
     token_copy(1, 0).wait_recv()
     route_far(2)
+    send_far(2, 0)
+    send_far(2, 1)
+    send_far(1, 1)
     pass_on(0)
     token_copy(2, 0).wait_recv()
     token_copy(2, 1).wait_recv()
     route_far(3)
+    send_far(3, 0)
+    send_far(3, 1)
     pass_on(1)
     for copy in loads:
         copy.wait()
@@ -512,7 +525,7 @@
 
     def home_copy(j, o):
         return pltpu.make_async_remote_copy(
-            src_ref=partial.at[j, pl.ds(3 * o, 3), :, far_cols],
+            src_ref=partial.at[j, pl.ds(3 * o, 3), :, far_back],
             dst_ref=far_answers.at[j, pl.ds(3 * sp, 3)],
             send_sem=home_send.at[j, o],
             recv_sem=home_recv.at[j, o],
@@ -535,12 +548,12 @@
 
         @pl.when(half == 0)
         def _():
-            far_answers[slot, pl.ds(3 * sp, 3)] = partial[slot, 0:3, :, NEAR:]
+            far_answers[slot, pl.ds(3 * sp, 3)] = partial[slot, 0:3, :, NEAR_BACK:]
 
     def sum_direct(slot, g):
         side = 0 if slot == 2 else 1
         return pltpu.make_async_remote_copy(
-            src_ref=partial.at[slot, group(g), :, near_cols],
+            src_ref=partial.at[slot, group(g), :, near_back],
             dst_ref=summed.at[side, group(g)],
             send_sem=sum_send.at[side, g],
             recv_sem=sum_recv.at[side, g],
@@ -550,7 +563,7 @@
 
     def sum_relay(g):
         return pltpu.make_async_remote_copy(
-            src_ref=partial.at[3, group(g), :, near_cols],
+            src_ref=partial.at[3, group(g), :, near_back],
             dst_ref=relayed.at[group(g)],
             send_sem=sum_send.at[2, g],
             recv_sem=sum_recv.at[2, g],
@@ -560,7 +573,7 @@
 
     def combine(j):
         each(1, 16, lambda o: home_copy(j, o).wait_recv())
-        flat = far_answers.at[j].reshape(16 * SLOTS, width - NEAR)
+        flat = far_answers.at[j].reshape(16 * SLOTS, width - NEAR_BACK)
         terms = dot(weighing[j], flat[...])
         return terms[0:TOK] + terms[TOK : 2 * TOK]
 
@@ -584,8 +597,8 @@
     def relay_add(g):
         slot = 2 if g < 2 else 1
         sum_relay(g).wait_recv()
-        partial[slot, group(g), :, 0:NEAR] = (
-            partial[slot, group(g), :, 0:NEAR].astype(F32) + relayed[group(g)].astype(F32)
+        partial[slot, group(g), :, 0:NEAR_BACK] = (
+            partial[slot, group(g), :, 0:NEAR_BACK].astype(F32) + relayed[group(g)].astype(F32)
         ).astype(BF16)
         sum_direct(slot, g).start()
 
@@ -622,7 +635,6 @@
         wait_far(1, 1)
 
     def before_across():
-        token_sum[...] = combine(0)
         onward(0).wait_recv()
         onward(1).wait_recv()
         wait_far(3, 0)
@@ -630,7 +642,6 @@
     def before_across_rest():
         sum_relay(0).start()
         sum_relay(1).start()
-        token_out[0] = combine(2).astype(BF16)
         onward(2).wait_recv()
         onward(3).wait_recv()
         wait_far(3, 1)
@@ -650,19 +661,18 @@
     each(0, 8, turn)
     sum_relay(2).start()
     sum_relay(3).start()
-    token_out[1] = combine(1).astype(BF16)
     relay_add(0)
     relay_add(2)
-    tsum_copy(0, 1).start()
-    tsum_copy(1, 0).start()
-    token_out[2] = combine(3).astype(BF16)
     relay_add(1)
     relay_add(3)
-    tsum_copy(2, 0).start()
-    tsum_copy(2, 1).start()
+    token_out[0] = combine(2).astype(BF16)
+    tsum_copy(0, 1).start()
+    token_out[1] = combine(1).astype(BF16)
+    tsum_copy(1, 0).start()
+
     def back(o):
         return pltpu.make_async_remote_copy(
-            src_ref=partial.at[0, pl.ds(3 * o, 3), :, near_cols],
+            src_ref=partial.at[0, pl.ds(3 * o, 3), :, near_back],
             dst_ref=answers.at[pl.ds(3 * sp, 3)],
             send_sem=back_send.at[o],
             recv_sem=back_recv.at[o],
@@ -670,18 +680,25 @@
             device_id_type=MESH,
         )
 
-    for g in (0, 2, 1, 3):
+    def settle(g):
         sum_direct(2, g).wait_recv()
         sum_direct(1, g).wait_recv()
-        partial[0, group(g), :, 0:NEAR] = (
-            partial[0, group(g), :, 0:NEAR].astype(F32)
+        partial[0, group(g), :, 0:NEAR_BACK] = (
+            partial[0, group(g), :, 0:NEAR_BACK].astype(F32)
             + summed[0, group(g)].astype(F32)
             + summed[1, group(g)].astype(F32)
         ).astype(BF16)
         each(max(4 * g, 1), 4 * g + 4, lambda o: back(o).start())
         if g == 0:
-            answers[pl.ds(3 * sp, 3)] = partial[0, 0:3, :, 0:NEAR]
-
+            answers[pl.ds(3 * sp, 3)] = partial[0, 0:3, :, 0:NEAR_BACK]
+
+    settle(0)
+    settle(2)
+    token_out[2] = combine(3).astype(BF16)
+    tsum_copy(2, 0).start()
+    tsum_copy(2, 1).start()
+    settle(1)
+    settle(3)
     for half in range(2):
         lane, rows = half, pl.ds(64 * half, 64)
         tsum_copy(2, half).wait_recv()
@@ -690,6 +707,7 @@
         ).astype(BF16)
         tsum_copy(lane, half).start()
 
+    token_sum[...] = combine(0)
     for copy in rims + notes:
         copy.wait_send()
     for lane in range(3):
@@ -698,8 +716,8 @@
             tsum_copy(lane, half).wait_send()
             if lane < 2:
                 tsum_copy(lane, half).wait_recv()
-    result[:, NEAR:] = (
-        normed[:, NEAR:].astype(F32)
+    result[:, NEAR_BACK:] = (
+        normed[:, NEAR_BACK:].astype(F32)
         + token_sum[...]
         + token_in[0].astype(F32)
         + token_in[1].astype(F32)
@@ -727,15 +745,16 @@
         back(o).wait_recv()
 
     each(1, 16, drain)
-    flat_answers = answers.reshape(16 * SLOTS, NEAR)
-
-    def finish(k):
-        cols = pl.ds(pl.multiple_of(k * 256, 256), 256)
+    flat_answers = answers.reshape(16 * SLOTS, NEAR_BACK)
+
+    def finish(k, size):
+        cols = pl.ds(k, size)
         terms = dot(weighing[0], flat_answers[:, cols])
         routed = terms[0:TOK] + terms[TOK : 2 * TOK]
         result[:, cols] = (normed[:, cols].astype(F32) + routed).astype(BF16)
 
-    each(0, NEAR // 256, finish)
+    for k in range(0, NEAR_BACK, 512):
+        finish(k, min(512, NEAR_BACK - k))
 
 
 def per_device(
@@ -767,10 +786,10 @@
     scalars = pl.BlockSpec(memory_space=pltpu.SMEM)
     dma = pltpu.SemaphoreType.DMA
     rows = 2 * SLOTS
-    rest = width - NEAR
+    rest = width - NEAR_BACK
     out = pl.pallas_call(
         layer_kernel,
-        out_shape=jax.ShapeDtypeStruct((TOK, width), BF16),
+        out_shape=pltpu.VMEM((TOK, width), BF16),
         in_specs=[scalars] + [far] * 7 + [near] * 4 + [far] + [near] * 2 + [far] * 5,
         out_specs=near,
         scratch_shapes=[
@@ -798,9 +817,9 @@
             pltpu.VMEM((4, 16 * SLOTS, TOK), BF16),
             pltpu.VMEM((4, 2 * TOK, 16 * SLOTS), BF16),
             pltpu.VMEM((rows, 8, width), BF16),
-            pltpu.VMEM((rows, 8, NEAR), BF16),
-            pltpu.VMEM((3, TOK, rest), BF16),
-            pltpu.VMEM((3, rows, 8, rest), BF16),
+            pltpu.VMEM((rows, 8, NEAR_BACK), BF16),
+            pltpu.VMEM((3, TOK, width - NEAR), BF16),
+            pltpu.VMEM((3, rows, 8, width - NEAR), BF16),
             pltpu.VMEM((4, rows, 8, rest), BF16),
             pltpu.VMEM((TOK, rest), F32),
             pltpu.VMEM((3, TOK, rest), BF16),
@@ -808,8 +827,8 @@
             pltpu.VMEM((2, TOK, rest), BF16),
             pltpu.VMEM((4, rows, 8, width), BF16),
             pltpu.VMEM((4, rows, 8, width), BF16),
-            pltpu.VMEM((rows, 8, NEAR), BF16),
-            pltpu.VMEM((2, rows, 8, NEAR), BF16),
+            pltpu.VMEM((rows, 8, NEAR_BACK), BF16),
+            pltpu.VMEM((2, rows, 8, NEAR_BACK), BF16),
             pltpu.VMEM((width, 2 * part), BF16),
             pltpu.VMEM((width, 2 * part), BF16),
             pltpu.VMEM((2 * part, width), BF16),

time: 124 us -> 115 us (0.927)
  Pallas kernels: 121 us -> 114 us
    pallas_call x1, Pallas kernels: 121 us -> 114 us  [per_device(): pl.pallas_call(layer_kernel, out_shape=pltpu.VMEM((TOK, width), BF16), in...]
where the time goes in v4:
time: 115 us
  Pallas kernels  114 us (99%)
    pallas_call x1, Pallas kernels, per_device(): pl.pallas_call(layer_kernel, out_shape=pltpu.VMEM((TOK, width), BF16), in...  114 us

profile of v4, /device:TPU:0, one launch (start us, length us, event | category | flops | bytes accessed | tf_op | source)
XLA Modules:
  0.0 115.1 jit_solution(13595607819336423960)
XLA Ops:
  0.0 114.3 %layer.1 = bf16[128,2048]{1,0:T(8,128)(2,1)S(1)} custom-call(f32[16]{0:T(128)} %speed.1, bf16[128,2048]{1,0:T(8,128)(2,1)} %bitcast.24, bf16[128,1024]{1,0:T(8,128)(2,1)} %bitcast.25, bf16[16,8,1024]{2,1,0:T(8,128)(2,1)} %bitcast.26, bf16[16,8,256]{2,1,0:T(8,128)(2,1)} %bitcast.27, bf16[16,8,256]{2,1,0:T(8,128)(2,1)} %bitcast.28, f32[16,1,128]{2,1,0:T(1,128)} %bitcast.29, ...), custom_call_target="tpu_custom_call" | custom-call | tf_op jit(solution)/shard_map/layer/pallas_call | solution.py:790
  114.3 0.8 copy.22

commit v5 on v4

--- a/solution.py
+++ b/solution.py
@@ -11,23 +11,29 @@
 TOK = 128
 INNER = 1024
 SLOTS = 24
-NEAR = 1152
-NEAR_BACK = 1152
+NEAR = 1280
+NEAR_BACK = 1280
 rms_eps = 1e-06
 norm_eps = 1e-05
 BF16 = jnp.bfloat16
 F32 = jnp.float32
-EXACT = lax.Precision.HIGHEST
-
-
-def dot(a, b, precision=None):
-    return jnp.dot(a, b, preferred_element_type=F32, precision=precision)
-
-
-def dot_nt(a, b, precision=None):
-    return lax.dot_general(
-        a, b, (((1,), (1,)), ((), ())), preferred_element_type=F32, precision=precision
-    )
+
+
+def dot(a, b):
+    return jnp.dot(a, b, preferred_element_type=F32)
+
+
+def thirds(a):
+    parts = []
+    for _ in range(3):
+        part = a.astype(BF16)
+        parts.append(part)
+        a = a - part.astype(F32)
+    return jnp.concatenate(parts, axis=1)
+
+
+def dot_nt(a, b):
+    return lax.dot_general(a, b, (((1,), (1,)), ((), ())), preferred_element_type=F32)
 
 
 def iota(shape, dim):
@@ -35,10 +41,10 @@
 
 
 def layer_kernel(
-    speed, skip_in, valve_in, chan, hid, probe, step_in, fade_in, tap_x, tap_b, tap_c, group_gain, out_w,
-    gain, offset, ids, shares, gate_w, raise_w, lower_w,
+    speed_in, skip_in, valve_in, chan, hid, probe, step_in, fade_in, tap_x_in, tap_b_in, tap_c_in,
+    group_gain_in, out_w, gain_in, offset_in, ids, shares, gate_w, raise_w, lower_w,
     result,
-    skip, valve, joined, rim, steps_out, fades_out, steps, fades, names, parts, conv, state, decay, state_in, decay_in, entering,
+    speed, tap_x, tap_b, tap_c, group_gain, gain, offset, skip, valve, joined, rim, steps_out, fades_out, steps, fades, names, parts, conv, state, decay, state_in, decay_in, entering,
     entered, inside, out_v, pre, normed, placing, weighing, outgoing, answers,
     tokens, far_rows, far_answers, token_sum, token_out, token_relay, token_in,
     gathered, partial, relayed, summed, gate_v, raise_v, lower_v, hidden,
@@ -96,7 +102,14 @@
     own_loads.append(pltpu.make_async_copy(ids, names.at[0], load_sem.at[6]))
     own_loads.append(pltpu.make_async_copy(shares, parts.at[0], load_sem.at[7]))
     out_load = pltpu.make_async_copy(out_w, out_v, load_sem.at[5])
+    for k, (source, target) in enumerate(
+        ((tap_x_in, tap_x), (tap_b_in, tap_b), (tap_c_in, tap_c), (speed_in, speed))
+    ):
+        own_loads.append(pltpu.make_async_copy(source, target, load_sem.at[10 + k]))
     late_loads = [
+        pltpu.make_async_copy(group_gain_in, group_gain, load_sem.at[14]),
+        pltpu.make_async_copy(gain_in, gain, load_sem.at[15]),
+        pltpu.make_async_copy(offset_in, offset, load_sem.at[16]),
         pltpu.make_async_copy(skip_in, skip, load_sem.at[8]),
         pltpu.make_async_copy(valve_in, valve, load_sem.at[9]),
     ]
@@ -222,14 +235,21 @@
     later = iota((TOK, TOK), 0)
     sooner = iota((TOK, TOK), 1)
     causal = later >= sooner
-    triangle = causal.astype(F32)
-    cum_row = dot_nt(fading, triangle, EXACT)
-    cum_col = dot_nt(triangle, fading, EXACT)
-    step_col = dot_nt((later == sooner).astype(F32), step, EXACT)
-    spread = (lax.div(iota((HEADS, INNER), 1), HEAD_DIM) == iota((HEADS, INNER), 0)).astype(F32)
+    triangle = causal.astype(F32).astype(BF16)
+    triangle = jnp.concatenate([triangle] * 3, axis=1)
+    same = (later == sooner).astype(F32).astype(BF16)
+    fading_parts = thirds(fading)
+    cum_row = dot_nt(fading_parts, triangle)
+    cum_col = dot_nt(triangle, fading_parts)
+    step_col = dot_nt(jnp.concatenate([same] * 3, axis=1), thirds(step))
+    spread = (
+        (lax.div(iota((3 * HEADS, INNER), 1), HEAD_DIM) == lax.rem(iota((3 * HEADS, INNER), 0), HEADS))
+        .astype(F32)
+        .astype(BF16)
+    )
     last = cum_col[TOK - 1 : TOK]
-    tail_wide = dot(jnp.exp(last - cum_col) * step_col, spread, EXACT)
-    decay_wide = dot(jnp.broadcast_to(jnp.exp(last), (8, HEADS)), spread, EXACT)
+    tail_wide = dot(thirds(jnp.exp(last - cum_col) * step_col), spread)
+    decay_wide = dot(thirds(jnp.broadcast_to(jnp.exp(last), (8, HEADS))), spread)
     for k in range(4):
         decay[k] = decay_wide[0:1, 256 * k : 256 * k + 256]
     scaled = (conv[:, 0:INNER].astype(F32) * tail_wide).astype(BF16)
@@ -354,7 +374,7 @@
 
     each(1, 16, lambda o: enter_copy(o).start())
     entered[my_rows, my_cols] = entering[sp]
-    reach_wide = dot(jnp.exp(cum_col), spread, EXACT)
+    reach_wide = dot(thirds(jnp.exp(cum_col)), spread)
     each(1, 16, lambda o: enter_copy(o).wait_recv())
 
     for copy in late_loads:
@@ -432,22 +452,24 @@
     for k in range(width // 512):
         route(k)
 
-    def go(o):
-        return pltpu.make_async_remote_copy(
-            src_ref=outgoing.at[pl.ds(3 * ahead(o), 3)],
-            dst_ref=gathered.at[0, pl.ds(3 * o, 3)],
-            send_sem=go_send.at[o],
-            recv_sem=go_recv.at[o],
-            device_id=(ahead(o), dp),
-            device_id_type=MESH,
-        )
-
-    each(1, 16, lambda o: go(o).start())
-    gathered[0, 0:3] = outgoing[pl.ds(3 * sp, 3)]
-
     near_cols = pl.ds(0, NEAR)
     near_back = pl.ds(0, NEAR_BACK)
     far_back = pl.ds(NEAR_BACK, width - NEAR_BACK)
+
+    def go(o, side=0):
+        cols = (near_cols, far_cols)[side]
+        return pltpu.make_async_remote_copy(
+            src_ref=outgoing.at[pl.ds(3 * ahead(o), 3), :, cols],
+            dst_ref=gathered.at[0, pl.ds(3 * o, 3), :, cols],
+            send_sem=go_send.at[side, o],
+            recv_sem=go_recv.at[side, o],
+            device_id=(ahead(o), dp),
+            device_id_type=MESH,
+        )
+
+    each(1, 16, lambda o: go(o).start())
+    each(1, 16, lambda o: go(o, 1).start())
+    gathered[0, 0:3] = outgoing[pl.ds(3 * sp, 3)]
 
     def group(g):
         return pl.ds(12 * g, 12)
@@ -516,10 +538,13 @@
     send_far(3, 0)
     send_far(3, 1)
     pass_on(1)
+    pass_on(2)
+    pass_on(3)
     for copy in loads:
         copy.wait()
     for copy in gifts:
         copy.wait()
+    each(1, 8, lambda o: go(o, 1).wait_recv())
 
     tile = 256
 
@@ -603,8 +628,7 @@
         sum_direct(slot, g).start()
 
     def before_own():
-        pass_on(2)
-        pass_on(3)
+        each(8, 16, lambda o: go(o, 1).wait_recv())
         to_right(0).wait_recv()
         onward(0).start()
 
@@ -616,11 +640,11 @@
     def before_right():
         to_left(0).wait_recv()
         to_left(1).wait_recv()
-        wait_far(2, 0)
-
-    def before_right_rest():
         to_left(2).wait_recv()
         onward(2).start()
+        wait_far(2, 0)
+
+    def before_right_rest():
         to_left(3).wait_recv()
         onward(3).start()
         sum_direct(1, 0).start()
@@ -737,6 +761,7 @@
         state_copy(o).wait_send()
         enter_copy(o).wait_send()
         go(o).wait_send()
+        go(o, 1).wait_send()
         for j in range(4):
             if j > 0:
                 far_copy(j, o).wait_send()
@@ -783,16 +808,22 @@
     part = specialist_gating_matrices.shape[2]
     far = pl.BlockSpec(memory_space=pl.ANY)
     near = pl.BlockSpec(memory_space=pltpu.VMEM)
-    scalars = pl.BlockSpec(memory_space=pltpu.SMEM)
     dma = pltpu.SemaphoreType.DMA
     rows = 2 * SLOTS
     rest = width - NEAR_BACK
     out = pl.pallas_call(
         layer_kernel,
         out_shape=pltpu.VMEM((TOK, width), BF16),
-        in_specs=[scalars] + [far] * 7 + [near] * 4 + [far] + [near] * 2 + [far] * 5,
+        in_specs=[far] * 20,
         out_specs=near,
         scratch_shapes=[
+            pltpu.SMEM((HEADS,), F32),
+            pltpu.VMEM((4, INNER), F32),
+            pltpu.VMEM((4, 256), F32),
+            pltpu.VMEM((4, 256), F32),
+            pltpu.VMEM((1, INNER), F32),
+            pltpu.VMEM((1, width), F32),
+            pltpu.VMEM((1, width), F32),
             pltpu.VMEM((TOK, width), BF16),
             pltpu.VMEM((TOK, INNER), BF16),
             pltpu.VMEM((16, 8, 1536), BF16),
@@ -833,8 +864,8 @@
             pltpu.VMEM((width, 2 * part), BF16),
             pltpu.VMEM((2 * part, width), BF16),
             pltpu.VMEM((192, 2 * part), BF16),
-            dma((10,)), dma((3,)), dma((3,)), dma((2, 3)), dma((2, 3)), dma((2, 16)), dma((2, 16)), dma((2, 16)), dma((2, 16)),
-            dma((16,)), dma((16,)), dma((3,)), dma((3,)), dma((3,)), dma((16,)), dma((16,)),
+            dma((17,)), dma((3,)), dma((3,)), dma((2, 3)), dma((2, 3)), dma((2, 16)), dma((2, 16)), dma((2, 16)), dma((2, 16)),
+            dma((16,)), dma((16,)), dma((3,)), dma((3,)), dma((3,)), dma((2, 16)), dma((2, 16)),
             dma((3, 4)), dma((3, 4)), dma((3, 4)), dma((3, 4)), dma((16,)), dma((16,)),
             dma((3, 2)), dma((3, 2)), dma((3, 16)), dma((3, 16)), dma((4, 16)), dma((4, 16)),
             dma((3, 2)), dma((3, 2)),

time: 115 us -> 112 us (0.974)
  Pallas kernels: 114 us -> 111 us
    pallas_call x1, Pallas kernels: 114 us -> 111 us  [per_device(): pl.pallas_call(layer_kernel, out_shape=pltpu.VMEM((TOK, width), BF16), in...]
where the time goes in v5:
time: 112 us; the launch traced here: 111 us
  Pallas kernels  111 us (99%)
    pallas_call x1, Pallas kernels, per_device(): pl.pallas_call(layer_kernel, out_shape=pltpu.VMEM((TOK, width), BF16), in...  111 us

profile of v5, /device:TPU:0, one launch (start us, length us, event | category | flops | bytes accessed | tf_op | source)
XLA Modules:
  0.0 111.4 jit_solution(3663251153296741231)
XLA Ops:
  0.0 110.6 %layer.1 = bf16[128,2048]{1,0:T(8,128)(2,1)S(1)} custom-call(f32[16]{0:T(128)} %speed_in.1, bf16[128,2048]{1,0:T(8,128)(2,1)} %bitcast.24, bf16[128,1024]{1,0:T(8,128)(2,1)} %bitcast.25, bf16[16,8,1024]{2,1,0:T(8,128)(2,1)} %bitcast.26, bf16[16,8,256]{2,1,0:T(8,128)(2,1)} %bitcast.27, bf16[16,8,256]{2,1,0:T(8,128)(2,1)} %bitcast.28, f32[16,1,128]{2,1,0:T(1,128)} %bitcast.29, ...), custom_call_target="tpu_custom_call" | custom-call | tf_op jit(solution)/shard_map/layer/pallas_call | solution.py:814
  110.6 0.8 copy.22

commit v6 on v5

--- a/solution.py
+++ b/solution.py
@@ -252,6 +252,18 @@
     decay_wide = dot(thirds(jnp.broadcast_to(jnp.exp(last), (8, HEADS))), spread)
     for k in range(4):
         decay[k] = decay_wide[0:1, 256 * k : 256 * k + 256]
+    def decay_copy(o):
+        return pltpu.make_async_remote_copy(
+            src_ref=decay.at[lax.rem(ahead(o), 4)],
+            dst_ref=decay_in.at[sp],
+            send_sem=state_send.at[1, o],
+            recv_sem=state_recv.at[1, o],
+            device_id=(ahead(o), dp),
+            device_id_type=MESH,
+        )
+
+    each(1, 16, lambda o: decay_copy(o).start())
+    decay_in[sp] = decay[lax.rem(sp, 4)]
     scaled = (conv[:, 0:INNER].astype(F32) * tail_wide).astype(BF16)
     for q in range(2):
         b_pair = conv[:, INNER + 128 * q : INNER + 128 * q + 128]
@@ -276,24 +288,12 @@
             device_id_type=MESH,
         )
 
-    def decay_copy(o):
-        return pltpu.make_async_remote_copy(
-            src_ref=decay.at[lax.rem(ahead(o), 4)],
-            dst_ref=decay_in.at[sp],
-            send_sem=state_send.at[1, o],
-            recv_sem=state_recv.at[1, o],
-            device_id=(ahead(o), dp),
-            device_id_type=MESH,
-        )
-
     def send_state(o):
-        decay_copy(o).start()
         state_copy(o).start()
 
     each(1, 16, send_state)
     my_rows, my_cols = place_of(sp)
     state_in[sp] = state[my_rows, my_cols]
-    decay_in[sp] = decay[lax.rem(sp, 4)]
 
     low_half = iota((TOK, TOK), 1) < 64
     for q in range(2):
@@ -446,10 +446,10 @@
     flat_outgoing = outgoing.reshape(16 * SLOTS, width)
 
     def route(k):
-        cols = pl.ds(512 * k, 512)
+        cols = pl.ds(256 * k, 256)
         flat_outgoing[:, cols] = dot(placing[0], normed[:, cols]).astype(BF16)
 
-    for k in range(width // 512):
+    for k in range(NEAR // 256):
         route(k)
 
     near_cols = pl.ds(0, NEAR)
@@ -468,6 +468,8 @@
         )
 
     each(1, 16, lambda o: go(o).start())
+    for k in range(NEAR // 256, width // 256):
+        route(k)
     each(1, 16, lambda o: go(o, 1).start())
     gathered[0, 0:3] = outgoing[pl.ds(3 * sp, 3)]
 
@@ -716,11 +718,24 @@
         if g == 0:
             answers[pl.ds(3 * sp, 3)] = partial[0, 0:3, :, 0:NEAR_BACK]
 
-    settle(0)
-    settle(2)
     token_out[2] = combine(3).astype(BF16)
     tsum_copy(2, 0).start()
     tsum_copy(2, 1).start()
+    settle(0)
+    settle(2)
+
+    def drain_early(o):
+        step_copy(o, steps_out, steps, 0).wait_send()
+        step_copy(o, fades_out, fades, 1).wait_send()
+        decay_copy(o).wait_send()
+        state_copy(o).wait_send()
+        enter_copy(o).wait_send()
+        go(o).wait_send()
+        go(o, 1).wait_send()
+        for j in range(1, 4):
+            far_copy(j, o).wait_send()
+
+    each(1, 16, drain_early)
     settle(1)
     settle(3)
     for half in range(2):
@@ -754,22 +769,7 @@
         sum_direct(2, g).wait_send()
         sum_relay(g).wait_send()
 
-    def drain(o):
-        step_copy(o, steps_out, steps, 0).wait_send()
-        step_copy(o, fades_out, fades, 1).wait_send()
-        decay_copy(o).wait_send()
-        state_copy(o).wait_send()
-        enter_copy(o).wait_send()
-        go(o).wait_send()
-        go(o, 1).wait_send()
-        for j in range(4):
-            if j > 0:
-                far_copy(j, o).wait_send()
-            home_copy(j, o).wait_send()
-        back(o).wait_send()
-        back(o).wait_recv()
-
-    each(1, 16, drain)
+    each(1, 16, lambda o: back(o).wait_recv())
     flat_answers = answers.reshape(16 * SLOTS, NEAR_BACK)
 
     def finish(k, size):
@@ -780,6 +780,13 @@
 
     for k in range(0, NEAR_BACK, 512):
         finish(k, min(512, NEAR_BACK - k))
+
+    def drain(o):
+        for j in range(4):
+            home_copy(j, o).wait_send()
+        back(o).wait_send()
+
+    each(1, 16, drain)
 
 
 def per_device(

time: 112 us -> 111 us (level)
  no operation moved by 1% of the time
where the time goes in v6:
time: 111 us
  Pallas kernels  110 us (99%)
    pallas_call x1, Pallas kernels, per_device(): pl.pallas_call(layer_kernel, out_shape=pltpu.VMEM((TOK, width), BF16), in...  110 us

profile of v6, /device:TPU:0, one launch (start us, length us, event | category | flops | bytes accessed | tf_op | source)
XLA Modules:
  0.0 111.3 jit_solution(13520141225455089285)
XLA Ops:
  0.0 110.5 %layer.1 = bf16[128,2048]{1,0:T(8,128)(2,1)S(1)} custom-call(f32[16]{0:T(128)} %speed_in.1, bf16[128,2048]{1,0:T(8,128)(2,1)} %bitcast.24, bf16[128,1024]{1,0:T(8,128)(2,1)} %bitcast.25, bf16[16,8,1024]{2,1,0:T(8,128)(2,1)} %bitcast.26, bf16[16,8,256]{2,1,0:T(8,128)(2,1)} %bitcast.27, bf16[16,8,256]{2,1,0:T(8,128)(2,1)} %bitcast.28, f32[16,1,128]{2,1,0:T(1,128)} %bitcast.29, ...), custom_call_target="tpu_custom_call" | custom-call | tf_op jit(solution)/shard_map/layer/pallas_call | solution.py:821
  110.5 0.8 copy.22
